TPU v7x, 256 devices: a 4x2x16 block of a 4x16x16 slice. The times are simulated.
256 devices in a mesh: grp: 2 (over y), ep: 64 (over z, x), tp: 2 (over core).
Axes of the slice: x: 4, y: 2, z: 16, core: 2. Of those that a mesh axis runs over, the one named last changes fastest.
The devices are a block of a 4x16x16 slice.
Arguments:
- tokens: bfloat16 [12288, 2048], P(('grp', 'ep')), parts along dimension 0, may hold values from -6 to 6
- prior_state: float32 [2, 12288, 4096], P(None, ('grp', 'ep'), 'tp'), parts along dimension 1, may hold values from -6 to 6
- mix_gain: float32 [2048], replicated, may hold values from 0.1 to 1.9
- in_weight: bfloat16 [2048, 1024], P(None, 'tp'), may hold values from -0.125 to 0.125
- decay_rate: float32 [64, 64], P('tp'), may hold values from 0.2 to 20
- frequency: float32 [64, 64], P('tp'), may hold values from 0 to 12
- log_step: float32 [64], P('tp'), may hold values from -4.6 to 0
- input_map: float32 [2, 64, 64, 16], P(None, 'tp'), may hold values from -6 to 6
- output_map: float32 [2, 64, 16, 64], P(None, 'tp'), may hold values from -0.5 to 0.5
- skip_gain: float32 [1024], P('tp'), may hold values from -4 to 4
- out_weight: bfloat16 [1024, 2048], P('tp'), may hold values from -0.1875 to 0.1875
- channel_gain: float32 [2048], replicated, may hold values from 0.1 to 1.9
- expert_gate: bfloat16 [64, 2048, 512], P('ep', None, 'tp'), may hold values from -0.125 to 0.125
- expert_up: bfloat16 [64, 2048, 512], P('ep', None, 'tp'), may hold values from -0.125 to 0.125
- expert_down: bfloat16 [64, 512, 2048], P('ep', 'tp'), may hold values from -0.25 to 0.25
- shared_gate: bfloat16 [2048, 512], P(None, 'tp'), may hold values from -0.125 to 0.125
- shared_up: bfloat16 [2048, 512], P(None, 'tp'), may hold values from -0.125 to 0.125
- shared_down: bfloat16 [512, 2048], P('tp'), may hold values from -0.25 to 0.25
- routes: int32 [12288, 6], P(('grp', 'ep')), parts along dimension 0, may hold values from 0 to 63, all different within a row; in each aligned block of 96 rows (0 to 95, 96 to 191, ...) at most 13 rows name the same one
- route_weights: float32 [12288, 6], P(('grp', 'ep')), parts along dimension 0, may hold values from 0.05 to 0.8
Outputs:
- layer_out: bfloat16 [12288, 2048], P(('grp', 'ep'), 'tp'), parts along dimension 0
- new_state: float32 [2, 12288, 4096], P(None, ('grp', 'ep'), 'tp'), parts along dimension 1
There are 2 independent parts, one for each index of `grp`. A program takes and returns all parts, laid end to end along the dimension named above; an argument that names none is the same for every part. Nothing has to cross between parts.
Inputs may be any that keep to these rules, and one draw needn't show every extreme that they name: `routes`: each row names 6 different experts; among the rows of one index of ep no expert is named by more than 13 rows.
All inputs are finite; a program needn't handle non-finite values.
Results may differ from a plain program's by a relative error of at most 0.017.
Values may be sent and summed in bfloat16 or wider, within the bound.
A program may use at most 128 MiB of HBM per device.

v0:
```python
import jax
import jax.numpy as jnp
from jax import lax
from jax.sharding import PartitionSpec as P

norm_eps = 1e-06


def copy_for_each(value, axis):
    peers = lax.axis_size(axis)
    return lax.all_to_all(
        jnp.broadcast_to(value[None], (peers, *value.shape)), axis, 0, 0, tiled=True
    )


def of_everyone(value, axis):
    return copy_for_each(value, axis).astype(jnp.float32).sum(axis=0)


def in_blocks(value, dim, peers):
    before, after = (value.shape[:dim], value.shape[dim + 1 :])
    return jnp.moveaxis(value.reshape(*before, peers, -1, *after), dim, 0)


def summed_on_arrival(value, axis, dim):
    tiles = in_blocks(value, dim, lax.axis_size(axis))
    arrived = lax.all_to_all(tiles, axis, split_axis=0, concat_axis=0, tiled=True)
    return arrived.astype(jnp.float32).sum(axis=0)


def root_scale(activations, scale_gain):
    values = activations.astype(jnp.float32)
    factor = lax.rsqrt(jnp.mean(values * values, axis=-1, keepdims=True) + norm_eps)
    return (values * factor * scale_gain).astype(jnp.bfloat16)


def state_update(
    drive_rows, prior_state, decay_rate, frequency, log_step, input_map, output_map, skip_gain
):
    sequences = drive_rows.shape[0]
    groups = decay_rate.shape[0]
    driven = drive_rows.astype(jnp.float32).reshape(sequences, groups, -1)
    step_size = jnp.exp(log_step)[:, None]
    real_rate = -decay_rate
    magnitude = jnp.exp(real_rate * step_size)
    turn_real = magnitude * jnp.cos(frequency * step_size)
    turn_imag = magnitude * jnp.sin(frequency * step_size)
    denominator = real_rate * real_rate + frequency * frequency
    hold_real = ((turn_real - 1.0) * real_rate + turn_imag * frequency) / denominator
    hold_imag = (turn_imag * real_rate - (turn_real - 1.0) * frequency) / denominator
    push_real = jnp.einsum("sgh,gph->sgp", driven, input_map[0])
    push_imag = jnp.einsum("sgh,gph->sgp", driven, input_map[1])
    enter_real = push_real * hold_real - push_imag * hold_imag
    enter_imag = push_real * hold_imag + push_imag * hold_real
    old_real = prior_state[0].reshape(sequences, groups, -1)
    old_imag = prior_state[1].reshape(sequences, groups, -1)
    fresh_real = turn_real * old_real - turn_imag * old_imag + enter_real
    fresh_imag = turn_real * old_imag + turn_imag * old_real + enter_imag
    readout = jnp.einsum("ghp,sgp->sgh", output_map[0], fresh_real)
    readout = readout - jnp.einsum("ghp,sgp->sgh", output_map[1], fresh_imag)
    readout = readout.reshape(sequences, -1) + skip_gain * drive_rows.astype(jnp.float32)
    fresh = jnp.stack([fresh_real.reshape(sequences, -1), fresh_imag.reshape(sequences, -1)])
    return (readout, fresh)


def body(
    tokens,
    prior_state,
    mix_gain,
    in_weight,
    decay_rate,
    frequency,
    log_step,
    input_map,
    output_map,
    skip_gain,
    out_weight,
    channel_gain,
    expert_gate,
    expert_up,
    expert_down,
    shared_gate,
    shared_up,
    shared_down,
    routes,
    route_weights,
):
    normed = root_scale(tokens, mix_gain)
    drive_rows = jnp.dot(normed, in_weight, preferred_element_type=jnp.float32).astype(jnp.bfloat16)
    readout, new_state = state_update(
        drive_rows, prior_state, decay_rate, frequency, log_step, input_map, output_map, skip_gain
    )
    activated = jax.nn.gelu(readout).astype(jnp.bfloat16)
    partial_value = jnp.dot(activated, out_weight, preferred_element_type=jnp.float32)
    mixer_out = of_everyone(partial_value.astype(jnp.bfloat16), "tp").astype(jnp.float32)
    middle = (tokens.astype(jnp.float32) + mixer_out).astype(jnp.bfloat16)
    second_normed = root_scale(middle, channel_gain)
    shared_gval = jnp.dot(second_normed, shared_gate, preferred_element_type=jnp.float32)
    shared_uval = jnp.dot(second_normed, shared_up, preferred_element_type=jnp.float32)
    shared_hidden = (jax.nn.silu(shared_gval) * shared_uval).astype(jnp.bfloat16)
    shared_piece = jnp.dot(shared_hidden, shared_down, preferred_element_type=jnp.float32)
    shared_out = summed_on_arrival(shared_piece.astype(jnp.bfloat16), "tp", 1)
    experts = lax.axis_size("ep")
    seq_rows, top_count = routes.shape
    slot_cap = min(seq_rows, max(2, 3 * seq_rows * top_count // (2 * experts)))
    flat_routes = routes.reshape(-1)
    one_hot = (flat_routes[:, None] == jnp.arange(experts, dtype=jnp.int32)[None, :]).astype(
        jnp.int32
    )
    ranked = jnp.sum((jnp.cumsum(one_hot, axis=0) - one_hot) * one_hot, axis=1)
    slot_index = flat_routes * slot_cap + ranked
    placed = slot_index[:, None] == jnp.arange(experts * slot_cap, dtype=jnp.int32)[None, :]
    placed_rows = jnp.any(placed.reshape(seq_rows, top_count, experts * slot_cap), axis=1).astype(
        jnp.bfloat16
    )
    outgoing = lax.dot_general(
        placed_rows, second_normed, (((0,), (0,)), ((), ())), preferred_element_type=jnp.float32
    ).astype(jnp.bfloat16)
    outgoing = outgoing.reshape(experts, slot_cap, -1)
    half_cols = outgoing.shape[2] // lax.axis_size("tp")
    own_cols = lax.dynamic_slice_in_dim(outgoing, lax.axis_index("tp") * half_cols, half_cols, 2)
    arrived = lax.all_gather(
        lax.all_to_all(own_cols, "ep", split_axis=0, concat_axis=0, tiled=True),
        "tp",
        axis=2,
        tiled=True,
    )
    sources, count_items, full_width = arrived.shape
    expert_rows = arrived.reshape(sources * count_items, full_width)
    gate_val = jnp.dot(expert_rows, expert_gate[0], preferred_element_type=jnp.float32)
    up_val = jnp.dot(expert_rows, expert_up[0], preferred_element_type=jnp.float32)
    hidden = (jax.nn.silu(gate_val) * up_val).astype(jnp.bfloat16)
    piece = jnp.dot(hidden, expert_down[0], preferred_element_type=jnp.float32)
    summed = summed_on_arrival(
        piece.reshape(sources, count_items, full_width).astype(jnp.bfloat16), "tp", 2
    )
    returned = lax.all_to_all(
        summed.astype(jnp.bfloat16), "ep", split_axis=0, concat_axis=0, tiled=True
    )
    flat_back = returned.reshape(experts * slot_cap, -1)
    picked = (
        jnp.take(flat_back, slot_index, axis=0).reshape(seq_rows, top_count, -1).astype(jnp.float32)
    )
    routed = jnp.einsum("sk,skd->sd", route_weights, picked)
    own_middle = lax.dynamic_slice_in_dim(middle, lax.axis_index("tp") * half_cols, half_cols, 1)
    layer_out = (own_middle.astype(jnp.float32) + routed + shared_out).astype(jnp.bfloat16)
    return (layer_out, new_state)


def solution(mesh):
    in_specs = (
        P(("grp", "ep"), None),
        P(None, ("grp", "ep"), "tp"),
        P(),
        P(None, "tp"),
        P("tp", None),
        P("tp", None),
        P("tp"),
        P(None, "tp", None, None),
        P(None, "tp", None, None),
        P("tp"),
        P("tp", None),
        P(),
        P("ep", None, "tp"),
        P("ep", None, "tp"),
        P("ep", "tp", None),
        P(None, "tp"),
        P(None, "tp"),
        P("tp", None),
        P(("grp", "ep"), None),
        P(("grp", "ep"), None),
    )
    out_specs = (P(("grp", "ep"), "tp"), P(None, ("grp", "ep"), "tp"))
    return jax.shard_map(body, mesh=mesh, in_specs=in_specs, out_specs=out_specs, check_vma=False)
```

profile of v0, /device:TPU:40, one launch (start us, length us, event | category | flops | bytes accessed | tf_op | source)
XLA Modules:
  0.0 344.0 jit_solution(5603154047995699530)
XLA Ops:
  7.2 0.8 exp.14
  8.0 1.2 fusion.13
  9.2 2.3 convolution_convert_fusion.4
  11.5 0.1 copy.91
  11.6 2.7 fusion.72
  14.3 1.5 copy.89
  15.8 2.5 copy.90
  18.2 1.4 fusion.29
  19.6 0.2 cosine_multiply_fusion
  19.8 3.0 bitcast_add_fusion
  22.9 0.2 fusion.25
  23.1 0.7 copy-done.2
  23.8 0.2 convolution_subtract_fusion
  24.1 0.1 copy-done.4
  24.2 0.1 copy.92
  24.4 0.5 convolution_convert_fusion.3
  24.8 1.0 broadcast_in_dim.9
  25.8 3.7 %all-to-all-start = ((bf16[2,96,2048]{2,1,0:T(8,128)(2,1)}), bf16[2,96,2048]{2,1,0:T(8,128)(2,1)S(1)}, u32[]{:S(2)}, u32[]{:S(2)}) async-start(bf16[2,96,2048]{2,1,0:T(8,128)(2,1)} %broadcast_in_dim.9), calls=%async_computation | async-start | bytes 1572864 | tf_op jit(solution)/shard_map/all_to_all | solution.py:11
  29.5 0.1 all-gather.2.cloned.1.call-start
  29.6 0.1 copy.93
  29.7 0.1 reshape.125
  29.9 1.5 reduce-window.6
  31.4 0.3 slice_reduce_fusion
  31.7 0.1 bitcast_bitcast_fusion.2
  31.9 0.1 reduce_sum.64
  32.0 0.1 copy.96
  32.1 0.3 fusion
  32.5 0.1 convert_reduce_fusion
  32.6 0.2 fusion.10
  32.8 0.7 copy-done.6
  33.6 1.1 convolution_convert_fusion.1
  34.7 2.9 reshape.128
  37.6 1.8 constant_dynamic-slice_fusion
  39.4 128.3 %all_to_all.25 = bf16[64,13,1024]{2,1,0:T(8,128)(2,1)} all-to-all(bf16[64,13,1024]{2,1,0:T(8,128)(2,1)S(1)} %constant_dynamic-slice_fusion), channel_id=1, replica_groups=mesh['grp'=2,'ep'=64,'tp'=2] {'ep'}, dimensions={0} | all-to-all | bytes 3407872 | tf_op jit(solution)/shard_map/all_to_all | solution.py:123
  167.7 0.9 copy-done.7
  168.7 1.6 fusion.67
  170.2 0.8 convolution_convert_fusion.2
  171.1 0.8 copy.121
  171.8 10.2 %all-gather.2.cloned.1.call-done = bf16[64,13,2048]{2,1,0:T(8,128)(2,1)} async-done(((bf16[64,13,1024]{2,1,0:T(8,128)(2,1)}), bf16[64,13,2048]{2,1,0:T(8,128)(2,1)}) %all-gather.2.cloned.1.call-update) | async-done | bytes 3407888 | tf_op jit(solution)/shard_map/all_gather | solution.py:122
  182.0 3.4 %reshape.129 = bf16[832,2048]{1,0:T(8,128)(2,1)S(1)} reshape(bf16[64,13,2048]{2,1,0:T(8,128)(2,1)} %all-gather.2.cloned.1.call-done) | data formatting | bytes 6815744 | tf_op jit(solution)/shard_map/reshape | solution.py:129
  185.5 2.4 fusion.8
  187.8 1.8 fusion.4
  189.7 1.2 dot_general.53
  190.8 2.3 convolution_convert_fusion
  193.1 0.5 copy.120
  193.6 6.5 %all_to_all.26 = bf16[2,64,13,1024]{3,1,2,0:T(8,128)(2,1)S(1)} all-to-all(bf16[2,64,13,1024]{3,1,2,0:T(8,128)(2,1)S(1)} %bitcast.84), channel_id=1, replica_groups=mesh['grp'=2,'ep'=64,'tp'=2] {'tp'}, dimensions={0} | all-to-all | bytes 6815744 | tf_op jit(solution)/shard_map/all_to_all | solution.py:27
  200.1 4.2 %all-to-all-start.4 = ((bf16[2,96,1024]{2,1,0:T(8,128)(2,1)}), bf16[2,96,1024]{2,1,0:T(8,128)(2,1)}, u32[]{:S(2)}, u32[]{:S(2)}) async-start(bf16[2,96,1024]{2,1,0:T(8,128)(2,1)} %bitcast.89), calls=%async_computation.4 | async-start | bytes 786432 | tf_op jit(solution)/shard_map/all_to_all | solution.py:27
  204.3 2.5 reduce_sum.66
  206.8 3.7 %copy.101 = bf16[64,13,1024]{2,1,0:T(8,128)(2,1)} copy(bf16[64,13,1024]{2,0,1:T(8,128)(2,1)} %reduce_sum.66) | data formatting | bytes 3407872 | tf_op jit(solution)/shard_map/reduce_sum | solution.py:28
  210.5 17.5 %all-to-all-start.3 = ((bf16[64,13,1024]{2,1,0:T(8,128)(2,1)}), bf16[64,13,1024]{2,1,0:T(8,128)(2,1)}, u32[]{:S(2)}, u32[]{:S(2)}) async-start(bf16[64,13,1024]{2,1,0:T(8,128)(2,1)} %copy.101), calls=%async_computation.3 | async-start | bytes 4194304 | tf_op jit(solution)/shard_map/all_to_all | solution.py:137
  228.1 0.1 copy.102
  228.2 0.1 mul.260
  228.3 0.1 copy.106
  228.5 0.1 copy.97
  228.6 0.3 copy.104
  228.9 0.3 copy.105
  229.3 1.8 convert_reduce_fusion.1
  231.1 1.2 pad_maximum_fusion
  232.4 94.9 %all-to-all-done.3 = bf16[64,13,1024]{2,1,0:T(8,128)(2,1)} async-done(((bf16[64,13,1024]{2,1,0:T(8,128)(2,1)}), bf16[64,13,1024]{2,1,0:T(8,128)(2,1)}, u32[]{:S(2)}, u32[]{:S(2)}) %all-to-all-start.3) | async-done | bytes 1703968 | tf_op jit(solution)/shard_map/all_to_all | solution.py:137
  327.3 2.6 reshape.131
  329.9 2.9 gather_fusion
  332.8 1.4 gather.7
  334.2 2.1 fusion.1
  336.3 0.8 fusion.21
  (53 shorter events, 0.3 us)
Async XLA Ops:
  7.2 17.1 %copy-start = (bf16[512,2048]{1,0:T(8,128)(2,1)S(1)}, bf16[512,2048]{1,0:T(8,128)(2,1)}, u32[]{:S(2)}) copy-start(bf16[512,2048]{1,0:T(8,128)(2,1)} %param.30) | copy-start | bytes 6291460
  15.7 3.9 %copy-start.17 = (f32[32,64]{1,0:T(8,128)S(1)}, f32[32,64]{1,0:T(8,128)}, u32[]{:S(2)}) copy-start(f32[32,64]{1,0:T(8,128)} %param.25) | copy-start | bytes 24580
  15.7 3.9 %copy-start.18 = (f32[32,64]{1,0:T(8,128)S(1)}, f32[32,64]{1,0:T(8,128)}, u32[]{:S(2)}) copy-start(f32[32,64]{1,0:T(8,128)} %param.24) | copy-start | bytes 24580
  18.2 1.6 copy-start.9
  19.8 3.1 copy-start.14
  22.8 1.0 copy-start.2
  22.9 1.3 copy-start.4
  22.9 1.5 copy-start.20
  24.3 5.3 %copy-start.16 = (s32[96,6]{0,1:T(8,128)S(1)}, s32[96,6]{0,1:T(8,128)}, u32[]{:S(2)}) copy-start(s32[96,6]{0,1:T(8,128)} %param.38) | copy-start | bytes 6916
  25.8 6.8 %copy-start.10 = (bf16[96,2048]{1,0:T(8,128)(2,1)S(1)}, bf16[96,2048]{1,0:T(8,128)(2,1)}, u32[]{:S(2)}) copy-start(bf16[96,2048]{1,0:T(8,128)(2,1)} %param.20) | copy-start | bytes 1179652
  25.8 6.6 %all-to-all-start = ((bf16[2,96,2048]{2,1,0:T(8,128)(2,1)}), bf16[2,96,2048]{2,1,0:T(8,128)(2,1)S(1)}, u32[]{:S(2)}, u32[]{:S(2)}) async-start(bf16[2,96,2048]{2,1,0:T(8,128)(2,1)} %broadcast_in_dim.9), calls=%async_computation | async-start | bytes 1572864 | tf_op jit(solution)/shard_map/all_to_all | solution.py:11
  29.5 152.5 %all-gather.2.cloned.1.call-start = ((), (), s32[]{:S(2)}) async-start(), calls=%async_computation.5 | async-start | bytes 6291456 | tf_op jit(solution)/shard_map/all_gather | solution.py:122
  31.4 2.1 copy-start.15
  32.8 0.7 copy-start.6
  167.7 1.0 copy-start.7
  167.7 2.6 copy-start.12
  167.7 2.6 copy-start.13
  185.5 2.4 copy-start.21
  200.1 10.4 %all-to-all-start.4 = ((bf16[2,96,1024]{2,1,0:T(8,128)(2,1)}), bf16[2,96,1024]{2,1,0:T(8,128)(2,1)}, u32[]{:S(2)}, u32[]{:S(2)}) async-start(bf16[2,96,1024]{2,1,0:T(8,128)(2,1)} %bitcast.89), calls=%async_computation.4 | async-start | bytes 786432 | tf_op jit(solution)/shard_map/all_to_all | solution.py:27
  210.5 17.8 %copy-start.19 = (f32[96,6]{0,1:T(8,128)S(1)}, f32[96,6]{0,1:T(8,128)}, u32[]{:S(2)}) copy-start(f32[96,6]{0,1:T(8,128)} %param.39) | copy-start | bytes 6916
  210.5 18.1 %copy-start.5 = (f32[96,32,64]{0,2,1:T(8,128)S(1)}, f32[96,32,64]{0,2,1:T(8,128)}, u32[]{:S(2)}) copy-start(f32[96,32,64]{0,2,1:T(8,128)} %copy-done.4) | copy-start | bytes 2359300
  210.5 18.4 %copy-start.3 = (f32[96,32,64]{0,2,1:T(8,128)S(1)}, f32[96,32,64]{0,2,1:T(8,128)}, u32[]{:S(2)}) copy-start(f32[96,32,64]{0,2,1:T(8,128)} %copy-done.2) | copy-start | bytes 2359300
  210.5 116.8 %all-to-all-start.3 = ((bf16[64,13,1024]{2,1,0:T(8,128)(2,1)}), bf16[64,13,1024]{2,1,0:T(8,128)(2,1)}, u32[]{:S(2)}, u32[]{:S(2)}) async-start(bf16[64,13,1024]{2,1,0:T(8,128)(2,1)} %copy.101), calls=%async_computation.3 | async-start | bytes 4194304 | tf_op jit(solution)/shard_map/all_to_all | solution.py:137
  332.8 4.3 %copy-start.1 = (bf16[512,2048]{1,0:T(8,128)(2,1)S(1)}, bf16[512,2048]{1,0:T(8,128)(2,1)}, u32[]{:S(2)}) copy-start(bf16[512,2048]{1,0:T(8,128)(2,1)} %param.30) | copy-start | bytes 6291460
  334.2 2.1 copy-start.8
  334.2 2.1 copy-start.11
Sparse Core Ops, SparseCore 0:
  167.8 14.1 all-gather.1
where the time goes:
time: 346 us; the launch traced here: 344 us
  blocking collectives  135 us (39%)
  waiting for transfers between devices  105 us (30%)
  local copies, waits for them, and re-layouts  34.1 us (10%)
  starting transfers between devices  25.5 us (7%)
  matrix products  19.7 us (6%)
  between operations  14.6 us (4%)
  other arithmetic  10.2 us (3%)
    all_to_all x1, blocking collectives, body(): lax.all_to_all(own_cols, 'ep', split_axis=0, concat_axis=0, tiled=True)  128 us
    all_to_all x1, waiting for transfers between devices, body(): lax.all_to_all(summed.astype(jnp.bfloat16), 'ep', split_axis=0, concat_ax...  94.9 us
    all_to_all x1, starting transfers between devices, body(): lax.all_to_all(summed.astype(jnp.bfloat16), 'ep', split_axis=0, concat_ax...  17.5 us
    all_gather x1, waiting for transfers between devices, body(): lax.all_gather(lax.all_to_all(own_cols, 'ep', split_axis=0, concat_axis=0...  10.2 us
  transfers between devices with their start and end apart: 4, of which 2 were waited for; matrix products, arithmetic and copies ran while one was open for 5% of the time, Pallas kernels for 0%

commit v1 on v0

--- a/solution.py
+++ b/solution.py
@@ -1,9 +1,383 @@
+import functools
+
 import jax
 import jax.numpy as jnp
 from jax import lax
+from jax.experimental import pallas as pl
+from jax.experimental.pallas import tpu as pltpu
 from jax.sharding import PartitionSpec as P
 
+MESH = pl.DeviceIdType.MESH
 norm_eps = 1e-06
+ROW_RING = 4
+CHUNKS = 4
+LANES = 128
+
+
+def moe_kernel(
+    cfg,
+    tokens_ref,
+    base_ref,
+    table_ref,
+    gate_hbm,
+    up_hbm,
+    down_hbm,
+    out_ref,
+    gathered,
+    tables,
+    codes,
+    shares,
+    pick,
+    spread,
+    staged,
+    rows_in,
+    w_in,
+    w_out,
+    partial,
+    partner_part,
+    total,
+    back,
+    sums_in,
+    sums_out,
+    w_sem,
+    t_send,
+    t_recv,
+    z_send,
+    z_recv,
+    x_send,
+    x_recv,
+    c_send,
+    c_recv,
+    p_send,
+    p_recv,
+    b_send,
+    b_recv,
+    r_send,
+    r_recv,
+):
+    Z, X, S, H, R, nc, top = cfg
+    W = H // nc
+    half = Z // 2
+    F = gate_hbm.shape[2]
+    ep = lax.axis_index("ep")
+    tp = lax.axis_index("tp")
+    other = 1 - tp
+    z, x = ep // X, lax.rem(ep, X)
+
+    def at_z(offset):
+        return {"ep": lax.rem(z + offset + Z, Z) * X + x}
+
+    def at_x(offset):
+        return {"ep": z * X + lax.rem(x + offset + X, X)}
+
+    partner = {"tp": other}
+
+    def send(src, dst, s_sem, r_sem, device):
+        return pltpu.make_async_remote_copy(
+            src_ref=src, dst_ref=dst, send_sem=s_sem, recv_sem=r_sem,
+            device_id=device, device_id_type=MESH,
+        )
+
+    def weight_copies():
+        return (
+            pltpu.make_async_copy(gate_hbm.at[0], w_in.at[:, pl.ds(0, F)], w_sem.at[0]),
+            pltpu.make_async_copy(up_hbm.at[0], w_in.at[:, pl.ds(F, F)], w_sem.at[1]),
+            pltpu.make_async_copy(down_hbm.at[0], w_out, w_sem.at[2]),
+        )
+
+    for copy in weight_copies():
+        copy.start()
+
+    barrier = pltpu.get_barrier_semaphore()
+    for k in range(1, Z):
+        pl.semaphore_signal(barrier, inc=1, device_id=at_z(k), device_id_type=MESH)
+    for d in range(1, X):
+        pl.semaphore_signal(barrier, inc=1, device_id=at_x(d), device_id_type=MESH)
+    pl.semaphore_signal(barrier, inc=1, device_id=partner, device_id_type=MESH)
+
+    tables[0] = table_ref[...]
+    for c in range(nc):
+        gathered[0, c] = tokens_ref[:, pl.ds(pl.multiple_of(tp * H + c * W, W), W)]
+
+    pl.semaphore_wait(barrier, Z + X - 1)
+
+    def table_copy(k):
+        return send(table_ref, tables.at[k], t_send.at[k], t_recv.at[k], at_z(k))
+
+    for k in range(1, Z):
+        table_copy(k).start()
+
+    def z_copy(way, k, c):
+        if way == 0:
+            return send(gathered.at[k, c], gathered.at[k + 1, c], z_send.at[0, k, c], z_recv.at[k + 1, c], at_z(1))
+        r = lax.rem(Z - k, Z)
+        return send(gathered.at[r, c], gathered.at[Z - k - 1, c], z_send.at[1, k, c], z_recv.at[Z - k - 1, c], at_z(-1))
+
+    def z_limit(way, c):
+        mine = (c < nc // 2) if way == 0 else (c >= nc // 2)
+        return half if mine else half - 1
+
+    def z_stage(k, c):
+        for way in (0, 1):
+            limit = z_limit(way, c)
+
+            @pl.when((k >= 1) & (k <= limit))
+            def _():
+                z_copy(way, k - 1, c).wait_recv()
+
+            @pl.when(k + 1 <= limit)
+            def _():
+                z_copy(way, k, c).start()
+
+    for c in range(nc):
+        z_stage(jnp.int32(0), c)
+
+    for k in range(1, Z):
+        table_copy(k).wait_recv()
+    before = (
+        lax.broadcasted_iota(jnp.int32, (LANES, LANES), 0) < lax.broadcasted_iota(jnp.int32, (LANES, LANES), 1)
+    ).astype(jnp.float32).astype(jnp.bfloat16)
+    for d in range(X):
+        expert = (z * X + lax.rem(x + d, X)).astype(jnp.float32)
+        named = jnp.zeros((Z, LANES), jnp.float32)
+        weight = jnp.zeros((Z, LANES), jnp.float32)
+        for k in range(top):
+            hit = tables[:, k, :] == expert
+            named = named + jnp.where(hit, 1.0, 0.0)
+            weight = weight + jnp.where(hit, tables[:, 8 + k, :], 0.0)
+        rank = jnp.dot(named.astype(jnp.bfloat16), before, preferred_element_type=jnp.float32)
+        codes[d] = jnp.where(named > 0.0, rank, -1.0)
+        shares[d] = weight
+
+    def build(r, carry):
+        slot = lax.broadcasted_iota(jnp.int32, (R, LANES), 0).astype(jnp.float32)
+        parts, weighted = [], []
+        for d in range(X):
+            block = jnp.where(codes[d, pl.ds(r, 1), :] == slot, 1.0, 0.0)
+            parts.append(block)
+            weighted.append(block * shares[d, pl.ds(r, 1), :])
+        pick[r] = jnp.concatenate(parts, axis=0).astype(jnp.bfloat16)
+        spread[r] = jnp.concatenate(weighted, axis=0).T.astype(jnp.bfloat16)
+        return carry
+
+    lax.fori_loop(0, Z, build, 0)
+    for copy in weight_copies():
+        copy.wait()
+
+    def x_copy(r, d):
+        rows = pl.ds(d * R, R)
+        return send(staged.at[r, :, rows, :], rows_in.at[r, tp, :, rows, :], x_send.at[r], x_recv.at[r], at_x(d))
+
+    def c_copy(r):
+        return send(rows_in.at[r, tp], rows_in.at[r, tp], c_send.at[r], c_recv.at[r], partner)
+
+    def p_copy(r):
+        return send(partial.at[r, other], partner_part.at[r], p_send.at[r], p_recv.at[r], partner)
+
+    def b_copy(r, d):
+        rows = pl.ds(d * R, R)
+        return send(total.at[r, :, rows, :], back.at[r, :, rows, :], b_send.at[r], b_recv.at[r], at_x(-d))
+
+    def select(r):
+        for c in range(nc):
+            chosen = jnp.dot(
+                pick[r, :, pl.ds(0, S)], gathered[r, c], preferred_element_type=jnp.float32
+            ).astype(jnp.bfloat16)
+            rows_in[r, tp, c, pl.ds(0, R), :] = chosen[:R]
+            staged[r, c] = chosen
+        for d in range(1, X):
+            x_copy(r, d).start()
+
+    rest = pl.ds(R, (X - 1) * R)
+
+    def hand_over(r):
+        send(staged.at[r, :, rest, :], rows_in.at[r, tp, :, rest, :], x_send.at[r], x_recv.at[r], at_x(1)).wait_recv()
+        c_copy(r).start()
+
+    def expert(r):
+        send(rows_in.at[r, other], rows_in.at[r, other], c_send.at[r], c_recv.at[r], partner).wait_recv()
+        acc = jnp.zeros((X * R, 2 * F), jnp.float32)
+        for h in range(2):
+            for c in range(nc):
+                acc = acc + jnp.dot(
+                    rows_in[r, h, c], w_in[pl.ds(h * H + c * W, W), :], preferred_element_type=jnp.float32
+                )
+        hidden = (jax.nn.silu(acc[:, :F]) * acc[:, F:]).astype(jnp.bfloat16)
+        for h in range(2):
+            for c in range(nc):
+                partial[r, h, c] = jnp.dot(
+                    hidden, w_out[:, pl.ds(h * H + c * W, W)], preferred_element_type=jnp.float32
+                ).astype(jnp.bfloat16)
+        p_copy(r).start()
+
+    def join(r):
+        p_copy(r).wait_recv()
+        for c in range(nc):
+            y = (partial[r, tp, c].astype(jnp.float32) + partner_part[r, c].astype(jnp.float32)).astype(jnp.bfloat16)
+            back[r, c, pl.ds(0, R), :] = y[:R]
+            total[r, c] = y
+        for d in range(1, X):
+            b_copy(r, d).start()
+
+    def of_pair(stage, k, way):
+        if way == 0:
+            @pl.when((k >= 0) & (k <= half))
+            def _():
+                stage(k)
+        else:
+            @pl.when((k >= 1) & (k < half))
+            def _():
+                stage(Z - k)
+
+    def step(i, carry):
+        z_stage(i, 0)
+        of_pair(select, i - 1, 0)
+        of_pair(select, i - 1, 1)
+        z_stage(i, 1)
+        of_pair(hand_over, i - 2, 0)
+        of_pair(hand_over, i - 2, 1)
+        of_pair(expert, i - 3, 0)
+        z_stage(i, 2)
+        of_pair(expert, i - 3, 1)
+        of_pair(join, i - 4, 0)
+        z_stage(i, 3)
+        of_pair(join, i - 4, 1)
+        return carry
+
+    lax.fori_loop(1, half + 5, step, 0)
+
+    def r_copy(way, k, c):
+        if way == 0:
+            return send(sums_out.at[k, c], sums_in.at[k - 1, c], r_send.at[k, c], r_recv.at[k - 1, c], at_z(-1))
+        return send(sums_out.at[Z - k, c], sums_in.at[Z - k + 1, c], r_send.at[Z - k, c], r_recv.at[Z - k + 1, c], at_z(1))
+
+    def share_of(r, c):
+        return jnp.dot(spread[r, pl.ds(0, S), :], back[r, c], preferred_element_type=jnp.float32)
+
+    def back_wait(r):
+        send(total.at[r, :, rest, :], back.at[r, :, rest, :], b_send.at[r], b_recv.at[r], at_x(1)).wait_recv()
+
+    def go_back(i, carry):
+        k = half - i
+        back_wait(k)
+
+        @pl.when(k < half)
+        def _():
+            back_wait(Z - k)
+
+        for c in range(nc):
+            for way in (0, 1):
+                limit = z_limit(way, c)
+                r = k if way == 0 else Z - k
+
+                @pl.when(k <= limit)
+                def _():
+                    mine = share_of(r, c)
+
+                    @pl.when(k == limit)
+                    def _():
+                        sums_out[r, c] = mine.astype(jnp.bfloat16)
+
+                    @pl.when(k < limit)
+                    def _():
+                        r_copy(way, k + 1, c).wait_recv()
+                        sums_out[r, c] = (mine + sums_in[r, c].astype(jnp.float32)).astype(jnp.bfloat16)
+
+                    r_copy(way, k, c).start()
+        return carry
+
+    lax.fori_loop(0, half, go_back, 0)
+
+    back_wait(0)
+    for c in range(nc):
+        mine = share_of(0, c) + base_ref[:, pl.ds(c * W, W)]
+        r_copy(0, 1, c).wait_recv()
+        r_copy(1, 1, c).wait_recv()
+        mine = mine + sums_in[0, c].astype(jnp.float32) + sums_in[Z, c].astype(jnp.float32)
+        out_ref[:, pl.ds(c * W, W)] = mine.astype(out_ref.dtype)
+
+    for k in range(1, Z):
+        table_copy(k).wait_send()
+
+    def drain(k, carry):
+        for c in range(nc):
+            for way in (0, 1):
+                limit = z_limit(way, c)
+
+                @pl.when(k + 1 <= limit)
+                def _():
+                    z_copy(way, k, c).wait_send()
+                    r_copy(way, k + 1, c).wait_send()
+        return carry
+
+    lax.fori_loop(0, half, drain, 0)
+
+    def drain_rows(r, carry):
+        send(staged.at[r, :, rest, :], rows_in.at[r, tp, :, rest, :], x_send.at[r], x_recv.at[r], at_x(1)).wait_send()
+        c_copy(r).wait_send()
+        p_copy(r).wait_send()
+        send(total.at[r, :, rest, :], back.at[r, :, rest, :], b_send.at[r], b_recv.at[r], at_x(1)).wait_send()
+        return carry
+
+    lax.fori_loop(0, Z, drain_rows, 0)
+
+
+def moe(tokens, base, table, gate, up, down, top):
+    S, D = tokens.shape
+    H = D // lax.axis_size("tp")
+    X = ROW_RING
+    Z = lax.axis_size("ep") // X
+    nc = CHUNKS
+    W = H // nc
+    R = 16
+    F = gate.shape[2]
+    bf, f4 = jnp.bfloat16, jnp.float32
+    dma = pltpu.SemaphoreType.DMA
+    vm = pl.BlockSpec(memory_space=pltpu.VMEM)
+    hb = pl.BlockSpec(memory_space=pl.ANY)
+    return pl.pallas_call(
+        functools.partial(moe_kernel, (Z, X, S, H, R, nc, top)),
+        out_shape=jax.ShapeDtypeStruct((S, H), bf),
+        in_specs=[vm, vm, vm, hb, hb, hb],
+        out_specs=vm,
+        scratch_shapes=[
+            pltpu.VMEM((Z, nc, S, W), bf),
+            pltpu.VMEM((Z, 16, LANES), f4),
+            pltpu.VMEM((X, Z, LANES), f4),
+            pltpu.VMEM((X, Z, LANES), f4),
+            pltpu.VMEM((Z, X * R, LANES), bf),
+            pltpu.VMEM((Z, LANES, X * R), bf),
+            pltpu.VMEM((Z, nc, X * R, W), bf),
+            pltpu.VMEM((Z, 2, nc, X * R, W), bf),
+            pltpu.VMEM((D, 2 * F), bf),
+            pltpu.VMEM((F, D), bf),
+            pltpu.VMEM((Z, 2, nc, X * R, W), bf),
+            pltpu.VMEM((Z, nc, X * R, W), bf),
+            pltpu.VMEM((Z, nc, X * R, W), bf),
+            pltpu.VMEM((Z, nc, X * R, W), bf),
+            pltpu.VMEM((Z + 1, nc, S, W), bf),
+            pltpu.VMEM((Z, nc, S, W), bf),
+            dma((3,)),
+            dma((Z,)),
+            dma((Z,)),
+            dma((2, Z // 2, nc)),
+            dma((Z, nc)),
+            dma((Z,)),
+            dma((Z,)),
+            dma((Z,)),
+            dma((Z,)),
+            dma((Z,)),
+            dma((Z,)),
+            dma((Z,)),
+            dma((Z,)),
+            dma((Z, nc)),
+            dma((Z + 1, nc)),
+        ],
+        compiler_params=pltpu.CompilerParams(
+            collective_id=0, has_side_effects=True, vmem_limit_bytes=48 * 1024 * 1024
+        ),
+        name="moe",
+    )(tokens, base, table, gate, up, down)
 
 
 def copy_for_each(value, axis):
@@ -100,50 +474,19 @@
     shared_hidden = (jax.nn.silu(shared_gval) * shared_uval).astype(jnp.bfloat16)
     shared_piece = jnp.dot(shared_hidden, shared_down, preferred_element_type=jnp.float32)
     shared_out = summed_on_arrival(shared_piece.astype(jnp.bfloat16), "tp", 1)
-    experts = lax.axis_size("ep")
+    half_cols = middle.shape[1] // lax.axis_size("tp")
+    own_middle = lax.dynamic_slice_in_dim(middle, lax.axis_index("tp") * half_cols, half_cols, 1)
+    base = own_middle.astype(jnp.float32) + shared_out
     seq_rows, top_count = routes.shape
-    slot_cap = min(seq_rows, max(2, 3 * seq_rows * top_count // (2 * experts)))
-    flat_routes = routes.reshape(-1)
-    one_hot = (flat_routes[:, None] == jnp.arange(experts, dtype=jnp.int32)[None, :]).astype(
-        jnp.int32
+    pad = ((0, 8 - top_count), (0, LANES - seq_rows))
+    table = jnp.concatenate(
+        [
+            jnp.pad(routes.T.astype(jnp.float32), pad, constant_values=-1.0),
+            jnp.pad(route_weights.T, pad),
+        ],
+        axis=0,
     )
-    ranked = jnp.sum((jnp.cumsum(one_hot, axis=0) - one_hot) * one_hot, axis=1)
-    slot_index = flat_routes * slot_cap + ranked
-    placed = slot_index[:, None] == jnp.arange(experts * slot_cap, dtype=jnp.int32)[None, :]
-    placed_rows = jnp.any(placed.reshape(seq_rows, top_count, experts * slot_cap), axis=1).astype(
-        jnp.bfloat16
-    )
-    outgoing = lax.dot_general(
-        placed_rows, second_normed, (((0,), (0,)), ((), ())), preferred_element_type=jnp.float32
-    ).astype(jnp.bfloat16)
-    outgoing = outgoing.reshape(experts, slot_cap, -1)
-    half_cols = outgoing.shape[2] // lax.axis_size("tp")
-    own_cols = lax.dynamic_slice_in_dim(outgoing, lax.axis_index("tp") * half_cols, half_cols, 2)
-    arrived = lax.all_gather(
-        lax.all_to_all(own_cols, "ep", split_axis=0, concat_axis=0, tiled=True),
-        "tp",
-        axis=2,
-        tiled=True,
-    )
-    sources, count_items, full_width = arrived.shape
-    expert_rows = arrived.reshape(sources * count_items, full_width)
-    gate_val = jnp.dot(expert_rows, expert_gate[0], preferred_element_type=jnp.float32)
-    up_val = jnp.dot(expert_rows, expert_up[0], preferred_element_type=jnp.float32)
-    hidden = (jax.nn.silu(gate_val) * up_val).astype(jnp.bfloat16)
-    piece = jnp.dot(hidden, expert_down[0], preferred_element_type=jnp.float32)
-    summed = summed_on_arrival(
-        piece.reshape(sources, count_items, full_width).astype(jnp.bfloat16), "tp", 2
-    )
-    returned = lax.all_to_all(
-        summed.astype(jnp.bfloat16), "ep", split_axis=0, concat_axis=0, tiled=True
-    )
-    flat_back = returned.reshape(experts * slot_cap, -1)
-    picked = (
-        jnp.take(flat_back, slot_index, axis=0).reshape(seq_rows, top_count, -1).astype(jnp.float32)
-    )
-    routed = jnp.einsum("sk,skd->sd", route_weights, picked)
-    own_middle = lax.dynamic_slice_in_dim(middle, lax.axis_index("tp") * half_cols, half_cols, 1)
-    layer_out = (own_middle.astype(jnp.float32) + routed + shared_out).astype(jnp.bfloat16)
+    layer_out = moe(second_normed, base, table, expert_gate, expert_up, expert_down, top_count)
     return (layer_out, new_state)
 
 

time: 346 us -> 181 us (0.52)
  Pallas kernels: 0 us -> 134 us
  blocking collectives: 135 us -> 4.51 us
  waiting for transfers between devices: 105 us -> 1.73 us
  starting transfers between devices: 25.5 us -> 4.2 us
  local copies, waits for them, and re-layouts: 34.1 us -> 17.6 us
  between operations: 14.6 us -> 0.96 us
  matrix products: 19.7 us -> 11.4 us
  other arithmetic: 10.2 us -> 6.67 us
    pallas_call x0 -> x1, Pallas kernels: none -> 134 us  [moe(): pl.pallas_call(functools.partial(moe_kernel, (Z, X, S, H, R, nc, top)), o...]
    all_to_all x2 -> x1, blocking collectives: 135 us -> 4.51 us  [copy_for_each(): lax.all_to_all(jnp.broadcast_to(value[None], (peers, *value.shape)), axis...]
    all_to_all x2 -> x0, waiting for transfers between devices: 94.9 us -> none  [the longest x1 94.9 us: body(): lax.all_to_all(summed.astype(jnp.bfloat16), 'ep', split_axis=0, concat_ax...]
    all_to_all x2 -> x0, starting transfers between devices: 21.2 us -> none  [the longest x1 17.5 us: body(): lax.all_to_all(summed.astype(jnp.bfloat16), 'ep', split_axis=0, concat_ax...]
    all_gather x1 -> x0, waiting for transfers between devices: 10.2 us -> none  [body(): lax.all_gather(lax.all_to_all(own_cols, 'ep', split_axis=0, concat_axis=0...]
    dot_general x5 -> x0, matrix products: 9.69 us -> none  [the longest x1 2.36 us: body(): jnp.dot(expert_rows, expert_gate[0], preferred_element_type=jnp.float32)]
    reshape x4 -> x0, local copies, waits for them, and re-layouts: 9.06 us -> none  [the longest x1 3.44 us: body(): expert_rows = arrived.reshape(sources * count_items, full_width)]
    gather x2 -> x0, local copies, waits for them, and re-layouts: 4.25 us -> none  [body(): jnp.take(flat_back, slot_index, axis=0).reshape(seq_rows, top_count, -1)]
  transfers between devices with their start and end apart: 4 -> 1, of which waited for: 2 -> 1; matrix products, arithmetic and copies ran while one was open for 5% -> 0% of each run, Pallas kernels for 0% -> 0%
where the time goes in v1:
time: 181 us
  Pallas kernels  134 us (74%)
  local copies, waits for them, and re-layouts  17.6 us (10%)
  matrix products  11.4 us (6%)
  other arithmetic  6.67 us (4%)
  blocking collectives  4.51 us (2%)
  starting transfers between devices  4.2 us (2%)
    pallas_call x1, Pallas kernels, moe(): pl.pallas_call(functools.partial(moe_kernel, (Z, X, S, H, R, nc, top)), o...  134 us
    all_to_all x1, blocking collectives, copy_for_each(): lax.all_to_all(jnp.broadcast_to(value[None], (peers, *value.shape)), axis...  4.51 us
    all_to_all x1, starting transfers between devices, summed_on_arrival(): lax.all_to_all(tiles, axis, split_axis=0, concat_axis=0, tiled=True)  4.2 us
    unnamed x43, local copies, waits for them, and re-layouts  4.19 us
    slice x2, local copies, waits for them, and re-layouts, state_update(): old_real = prior_state[0].reshape(sequences, groups, -1)  4.15 us
    another operation x2, local copies, waits for them, and re-layouts, state_update(): jnp.stack([fresh_real.reshape(sequences, -1), fresh_imag.reshape(sequence...  3.81 us
  transfers between devices with their start and end apart: 1, of which 1 were waited for; matrix products, arithmetic and copies ran while one was open for 0% of the time, Pallas kernels for 0%

profile of v1, /device:TPU:40, one launch (start us, length us, event | category | flops | bytes accessed | tf_op | source)
XLA Modules:
  0.0 180.6 jit_solution(2249857603023594695)
XLA Ops:
  0.6 0.0 copy-start
  0.6 0.8 exp.10
  1.5 1.2 fusion.4
  2.6 2.3 %convolution_convert_fusion.2 = bf16[96,512]{1,0:T(8,128)(2,1)S(1)} fusion(bf16[2048,512]{1,0:T(8,128)(2,1)} %param.23, bf16[96,2048]{1,0:T(8,128)(2,1)} %param.20, f32[2048]{0:T(1024)} %param.22, f32[96]{0:T(128)S(1)} %add_rsqrt_fusion.1), kind=kOutput, calls=%fused_computation.8 | convolution fusion | flops 202162176 | bytes 2597248 | tf_op jit(solution)/shard_map/dot_general | solution.py:463
  4.9 0.1 copy.44
  5.0 2.7 %fusion.48 = (f32[1,96,2048]{2,1,0:T(8,128)}, f32[1,96,2048]{2,1,0:T(8,128)}) fusion(f32[2,96,2048]{2,1,0:T(8,128)} %param.21), kind=kLoop, calls=%fused_computation.75 | loop fusion | bytes 3145728 | tf_op jit(solution)/shard_map/slice | solution.py:429
  7.7 1.5 copy.42
  9.2 0.0 copy-start.15
  9.2 0.0 copy-start.16
  9.2 2.5 %copy.43 = f32[1,96,2048]{1,2,0:T(8,128)} copy(f32[1,96,2048]{2,1,0:T(8,128)} %get-tuple-element.7) | data formatting | bytes 1572864 | tf_op jit(solution)/shard_map/slice | solution.py:430
  11.7 1.4 fusion.16
  13.1 0.0 copy-done.15
  13.1 0.0 copy-done.16
  13.1 0.2 cosine_multiply_fusion
  13.2 0.0 copy-done.9
  13.3 0.0 copy-start.14
  13.3 3.0 %bitcast_add_fusion = (f32[96,32,64]{0,2,1:T(8,128)S(1)}, f32[96,32,64]{0,2,1:T(8,128)S(1)}) fusion(f32[32,96,64]{1,2,0:T(8,128)S(1)} %fusion.16, f32[96,32,64]{0,2,1:T(8,128)S(1)} %bitcast.49, f32[96,32,64]{0,2,1:T(8,128)S(1)} %bitcast.50, f32[32,64]{1,0:T(8,128)S(1)} %get-tuple-element.10, f32[32,64]{1,0:T(8,128)S(1)} %get-tuple-element.9, ...), kind=kOutput, calls=%fused_computation.11 | convolution fusion | flops 9043968 | bytes 4194304 | tf_op jit(solution)/shard_map/sgh,gph->sgp/dot_general | solution.py:426
  16.3 0.0 copy-start.6
  16.3 0.0 copy-start.8
  16.3 0.0 copy-start.20
  16.3 0.0 copy-done.14
  16.4 0.2 fusion.12
  16.6 0.7 copy-done.6
  17.3 0.2 convolution_subtract_fusion
  17.5 0.1 copy-done.8
  17.6 0.1 copy.45
  17.8 0.0 copy-done
  17.8 0.0 copy-done.20
  17.8 0.5 convolution_convert_fusion.1
  18.3 0.0 copy-start.10
  18.3 0.1 broadcast_in_dim.2
  18.4 0.0 copy-start.17
  18.4 4.5 %all_to_all.10 = bf16[2,96,2048]{2,1,0:T(8,128)(2,1)S(1)} all-to-all(bf16[2,96,2048]{2,1,0:T(8,128)(2,1)S(1)} %broadcast_in_dim.2), channel_id=1, replica_groups=mesh['grp'=2,'ep'=64,'tp'=2] {'tp'}, dimensions={0} | all-to-all | bytes 1572864 | tf_op jit(solution)/shard_map/all_to_all | solution.py:385
  22.9 0.1 convert_reduce_fusion
  23.0 0.0 copy-done.10
  23.1 0.0 copy-start.12
  23.1 0.2 fusion.1
  23.3 0.7 copy-done.11
  24.0 0.0 copy-done.17
  24.0 0.2 fusion.3.tokens_ref
  24.2 0.0 copy-done.13
  24.2 1.0 fusion.49
  25.2 0.0 copy-done.12
  25.2 2.8 %convolution_convert_fusion = bf16[96,2048]{1,0:T(8,128)(2,1)} fusion(bf16[256,2048]{1,0:T(8,128)(2,1)S(1)} %copy-done.12, bf16[96,2048]{1,0:T(8,128)(2,1)S(1)} %fusion.3.tokens_ref, bf16[2048,256]{1,0:T(8,128)(2,1)} %param.36, f32[96,256]{1,0:T(8,128)} %fusion.49), kind=kOutput, calls=%fused_computation | convolution fusion | flops 201670656 | bytes 2981888 | tf_op jit(solution)/shard_map/dot_general | solution.py:475
  27.9 1.9 %copy.51 = bf16[12,2,8,1024]{3,2,0,1:T(8,128)(2,1)} copy(bf16[12,2,8,1024]{3,2,1,0:T(8,128)(2,1)} %bitcast.52) | data formatting | bytes 786432 | tf_op jit(solution)/shard_map/reshape | solution.py:396
  29.8 4.2 %all-to-all-start.1 = ((bf16[2,96,1024]{2,1,0:T(8,128)(2,1)}), bf16[2,96,1024]{2,1,0:T(8,128)(2,1)}, u32[]{:S(2)}, u32[]{:S(2)}) async-start(bf16[2,96,1024]{2,1,0:T(8,128)(2,1)} %bitcast.51), calls=%async_computation.1 | async-start | bytes 786432 | tf_op jit(solution)/shard_map/all_to_all | solution.py:401
  34.0 0.0 copy-done.18
  34.0 1.7 all-to-all-done.1
  35.8 1.2 convert_reduce_fusion.1
  37.0 1.0 convert_add_fusion.1.base_ref
  37.9 0.0 copy-done.19
  38.0 0.0 copy-done.1
  38.0 0.0 copy-done.2
  38.0 0.0 copy-start.3
  38.0 1.2 copy-done.3
  39.2 133.6 %moe.1 = bf16[96,1024]{1,0:T(8,128)(2,1)S(1)} custom-call(bf16[96,2048]{1,0:T(8,128)(2,1)S(1)} %fusion.3.tokens_ref, f32[96,1024]{1,0:T(8,128)S(1)} %convert_add_fusion.1.base_ref, f32[16,128]{1,0:T(8,128)S(1)} %select_maximum_fusion.table_ref, bf16[1,2048,256]{2,1,0:T(8,128)(2,1)S(1)} %copy-done.1, bf16[1,2048,256]{2,1,0:T(8,128)(2,1)S(1)} %copy-done.2, ...), custom_call_target="tpu_custom_call" | custom-call | tf_op jit(solution)/shard_map/moe/pallas_call | solution.py:338
  172.8 0.0 copy-start.4
  172.8 0.7 copy-done.4
  173.5 2.6 %copy.47 = f32[1,96,2048]{2,1,0:T(8,128)} copy(f32[1,96,2048]{1,2,0:T(8,128)} %bitcast.48) | data formatting | bytes 1572864 | tf_op jit(solution)/shard_map/stack;reshape | solution.py:436
  176.0 0.0 copy-done.7
  176.1 1.2 copy.48
  177.3 2.7 %pad_maximum_fusion = f32[2,96,2048]{2,1,0:T(8,128)} fusion(f32[1,96,2048]{2,1,0:T(8,128)} %copy.48, f32[1,96,2048]{2,1,0:T(8,128)} %copy.47), kind=kLoop, calls=%fused_computation.2 | loop fusion | flops 393216 | bytes 3145728 | tf_op jit(solution)/shard_map/stack | solution.py:436
  180.0 0.0 copy-done.5
  180.0 0.7 copy.53
  (13 shorter events, 0.0 us)
Async XLA Ops:
  0.6 17.1 %copy-start = (bf16[512,2048]{1,0:T(8,128)(2,1)S(1)}, bf16[512,2048]{1,0:T(8,128)(2,1)}, u32[]{:S(2)}) copy-start(bf16[512,2048]{1,0:T(8,128)(2,1)} %param.30) | copy-start | bytes 6291460
  9.2 3.9 %copy-start.15 = (f32[32,64]{1,0:T(8,128)S(1)}, f32[32,64]{1,0:T(8,128)}, u32[]{:S(2)}) copy-start(f32[32,64]{1,0:T(8,128)} %param.25) | copy-start | bytes 24580
  9.2 3.9 %copy-start.16 = (f32[32,64]{1,0:T(8,128)S(1)}, f32[32,64]{1,0:T(8,128)}, u32[]{:S(2)}) copy-start(f32[32,64]{1,0:T(8,128)} %param.24) | copy-start | bytes 24580
  11.7 1.6 copy-start.9
  13.3 3.1 %copy-start.14 = (f32[2,32,16,64]{3,2,1,0:T(8,128)S(1)}, f32[2,32,16,64]{3,2,1,0:T(8,128)}, u32[]{:S(2)}) copy-start(f32[2,32,16,64]{3,2,1,0:T(8,128)} %param.28) | copy-start | bytes 786436
  16.3 1.0 copy-start.6
  16.3 1.3 copy-start.8
  16.3 1.4 copy-start.20
  18.3 4.8 %copy-start.10 = (bf16[96,2048]{1,0:T(8,128)(2,1)S(1)}, bf16[96,2048]{1,0:T(8,128)(2,1)}, u32[]{:S(2)}) copy-start(bf16[96,2048]{1,0:T(8,128)(2,1)} %param.20) | copy-start | bytes 1179652
  18.4 5.7 %copy-start.17 = (f32[2048]{0:T(1024)S(1)}, f32[2048]{0:T(1024)}, u32[]{:S(2)}) copy-start(f32[2048]{0:T(1024)} %param.31) | copy-start | bytes 24580
  22.9 1.3 copy-start.13
  23.1 2.1 %copy-start.12 = (bf16[256,2048]{1,0:T(8,128)(2,1)S(1)}, bf16[256,2048]{1,0:T(8,128)(2,1)}, u32[]{:S(2)}) copy-start(bf16[256,2048]{1,0:T(8,128)(2,1)} %param.37) | copy-start | bytes 3145732
  23.3 0.8 copy-start.11
  25.2 8.9 %copy-start.18 = (s32[96,6]{0,1:T(8,128)S(1)}, s32[96,6]{0,1:T(8,128)}, u32[]{:S(2)}) copy-start(s32[96,6]{0,1:T(8,128)} %param.38) | copy-start | bytes 6916
  27.9 10.0 %copy-start.19 = (f32[96,6]{0,1:T(8,128)S(1)}, f32[96,6]{0,1:T(8,128)}, u32[]{:S(2)}) copy-start(f32[96,6]{0,1:T(8,128)} %param.39) | copy-start | bytes 6916
  27.9 10.0 %copy-start.1 = (bf16[1,2048,256]{2,1,0:T(8,128)(2,1)S(1)}, bf16[1,2048,256]{2,1,0:T(8,128)(2,1)}, u32[]{:S(2)}) copy-start(bf16[1,2048,256]{2,1,0:T(8,128)(2,1)} %gate_hbm.1) | copy-start | bytes 3145732
  29.8 6.0 %all-to-all-start.1 = ((bf16[2,96,1024]{2,1,0:T(8,128)(2,1)}), bf16[2,96,1024]{2,1,0:T(8,128)(2,1)}, u32[]{:S(2)}, u32[]{:S(2)}) async-start(bf16[2,96,1024]{2,1,0:T(8,128)(2,1)} %bitcast.51), calls=%async_computation.1 | async-start | bytes 786432 | tf_op jit(solution)/shard_map/all_to_all | solution.py:401
  35.8 2.2 %copy-start.2 = (bf16[1,2048,256]{2,1,0:T(8,128)(2,1)S(1)}, bf16[1,2048,256]{2,1,0:T(8,128)(2,1)}, u32[]{:S(2)}) copy-start(bf16[1,2048,256]{2,1,0:T(8,128)(2,1)} %up_hbm.1) | copy-start | bytes 3145732
  38.0 1.2 copy-start.3
  172.8 0.7 copy-start.4
  173.5 2.6 %copy-start.7 = (f32[96,32,64]{0,2,1:T(8,128)S(1)}, f32[96,32,64]{0,2,1:T(8,128)}, u32[]{:S(2)}) copy-start(f32[96,32,64]{0,2,1:T(8,128)} %copy-done.6) | copy-start | bytes 2359300
  176.1 3.9 %copy-start.5 = (bf16[96,1024]{1,0:T(8,128)(2,1)S(1)}, bf16[96,1024]{1,0:T(8,128)(2,1)}, u32[]{:S(2)}) copy-start(bf16[96,1024]{1,0:T(8,128)(2,1)} %copy-done.4) | copy-start | bytes 589828

commit v2 on v1

--- a/solution.py
+++ b/solution.py
@@ -14,19 +14,32 @@
 LANES = 128
 
 
-def moe_kernel(
+def layer_kernel(
     cfg,
+    active_ref,
     tokens_ref,
-    base_ref,
+    gain_ref,
     table_ref,
+    project_hbm,
+    sgate_hbm,
+    sup_hbm,
+    sdown_hbm,
     gate_hbm,
     up_hbm,
     down_hbm,
     out_ref,
+    project,
+    mixed,
+    mixed_in,
+    middle,
+    normed,
+    s_in,
+    s_out,
+    s_hidden,
+    s_part,
+    s_part_in,
     gathered,
     tables,
-    codes,
-    shares,
     pick,
     spread,
     staged,
@@ -40,6 +53,8 @@
     sums_in,
     sums_out,
     w_sem,
+    m_sem,
+    s_sem,
     t_send,
     t_recv,
     z_send,
@@ -59,6 +74,7 @@
     W = H // nc
     half = Z // 2
     F = gate_hbm.shape[2]
+    SF = sgate_hbm.shape[1]
     ep = lax.axis_index("ep")
     tp = lax.axis_index("tp")
     other = 1 - tp
@@ -78,34 +94,60 @@
             device_id=device, device_id_type=MESH,
         )
 
-    def weight_copies():
+    def project_copy():
+        return pltpu.make_async_copy(project_hbm, project, w_sem.at[0])
+
+    def shared_copies():
         return (
-            pltpu.make_async_copy(gate_hbm.at[0], w_in.at[:, pl.ds(0, F)], w_sem.at[0]),
-            pltpu.make_async_copy(up_hbm.at[0], w_in.at[:, pl.ds(F, F)], w_sem.at[1]),
-            pltpu.make_async_copy(down_hbm.at[0], w_out, w_sem.at[2]),
+            pltpu.make_async_copy(sgate_hbm, s_in.at[:, pl.ds(0, SF)], w_sem.at[1]),
+            pltpu.make_async_copy(sup_hbm, s_in.at[:, pl.ds(SF, SF)], w_sem.at[2]),
+            pltpu.make_async_copy(sdown_hbm, s_out, w_sem.at[3]),
         )
 
-    for copy in weight_copies():
+    def expert_copies():
+        return (
+            pltpu.make_async_copy(gate_hbm.at[0], w_in.at[:, pl.ds(0, F)], w_sem.at[4]),
+            pltpu.make_async_copy(up_hbm.at[0], w_in.at[:, pl.ds(F, F)], w_sem.at[5]),
+            pltpu.make_async_copy(down_hbm.at[0], w_out, w_sem.at[6]),
+        )
+
+    project_copy().start()
+
+    barrier = pltpu.get_barrier_semaphore()
+    for device in (at_z(1), at_z(-1), *[at_x(d) for d in range(1, X)], partner):
+        pl.semaphore_signal(barrier, inc=1, device_id=device, device_id_type=MESH)
+
+    tables[0] = table_ref[...]
+    project_copy().wait()
+    for copy in (*shared_copies(), *expert_copies()):
         copy.start()
-
-    barrier = pltpu.get_barrier_semaphore()
-    for k in range(1, Z):
-        pl.semaphore_signal(barrier, inc=1, device_id=at_z(k), device_id_type=MESH)
-    for d in range(1, X):
-        pl.semaphore_signal(barrier, inc=1, device_id=at_x(d), device_id_type=MESH)
-    pl.semaphore_signal(barrier, inc=1, device_id=partner, device_id_type=MESH)
-
-    tables[0] = table_ref[...]
-    for c in range(nc):
-        gathered[0, c] = tokens_ref[:, pl.ds(pl.multiple_of(tp * H + c * W, W), W)]
-
-    pl.semaphore_wait(barrier, Z + X - 1)
-
-    def table_copy(k):
-        return send(table_ref, tables.at[k], t_send.at[k], t_recv.at[k], at_z(k))
-
-    for k in range(1, Z):
-        table_copy(k).start()
+    active = active_ref[...]
+    for h in range(2 * nc):
+        cols = slice(h * W, (h + 1) * W)
+        mixed[:, cols] = jnp.dot(active, project[:, cols], preferred_element_type=jnp.float32).astype(jnp.bfloat16)
+
+    pl.semaphore_wait(barrier, X + 2)
+
+    mixed_copy = send(mixed, mixed_in, m_sem.at[0], m_sem.at[1], partner)
+    mixed_copy.start()
+
+    def t_copy(way, k):
+        if way == 0:
+            return send(tables.at[k], tables.at[k + 1], t_send.at[0, k], t_recv.at[k + 1], at_z(1))
+        r = lax.rem(Z - k, Z)
+        return send(tables.at[r], tables.at[Z - k - 1], t_send.at[1, k], t_recv.at[Z - k - 1], at_z(-1))
+
+    def t_stage(k):
+        for way in (0, 1):
+            limit = half - way
+
+            @pl.when((k >= 1) & (k <= limit))
+            def _():
+                t_copy(way, k - 1).wait_recv()
+
+            @pl.when(k + 1 <= limit)
+            def _():
+                t_copy(way, k).start()
 
     def z_copy(way, k, c):
         if way == 0:
@@ -129,40 +171,65 @@
             def _():
                 z_copy(way, k, c).start()
 
-    for c in range(nc):
-        z_stage(jnp.int32(0), c)
-
-    for k in range(1, Z):
-        table_copy(k).wait_recv()
     before = (
         lax.broadcasted_iota(jnp.int32, (LANES, LANES), 0) < lax.broadcasted_iota(jnp.int32, (LANES, LANES), 1)
     ).astype(jnp.float32).astype(jnp.bfloat16)
-    for d in range(X):
-        expert = (z * X + lax.rem(x + d, X)).astype(jnp.float32)
-        named = jnp.zeros((Z, LANES), jnp.float32)
-        weight = jnp.zeros((Z, LANES), jnp.float32)
+    offset = lax.broadcasted_iota(jnp.int32, (8, LANES), 0)
+    column = offset + x
+    column = jnp.where(column >= X, column - X, column)
+    expert_of = jnp.where(offset < X, z * X + column, -2).astype(jnp.float32)
+
+    def build(r):
+        table = tables[r].astype(jnp.float32)
+        named = jnp.zeros((8, LANES), jnp.float32)
+        weight = jnp.zeros((8, LANES), jnp.float32)
         for k in range(top):
-            hit = tables[:, k, :] == expert
+            hit = table[k : k + 1, :] == expert_of
             named = named + jnp.where(hit, 1.0, 0.0)
-            weight = weight + jnp.where(hit, tables[:, 8 + k, :], 0.0)
+            weight = weight + jnp.where(hit, table[8 + k : 9 + k, :], 0.0)
         rank = jnp.dot(named.astype(jnp.bfloat16), before, preferred_element_type=jnp.float32)
-        codes[d] = jnp.where(named > 0.0, rank, -1.0)
-        shares[d] = weight
-
-    def build(r, carry):
+        code = jnp.where(named > 0.0, rank, -1.0)
         slot = lax.broadcasted_iota(jnp.int32, (R, LANES), 0).astype(jnp.float32)
         parts, weighted = [], []
         for d in range(X):
-            block = jnp.where(codes[d, pl.ds(r, 1), :] == slot, 1.0, 0.0)
+            block = jnp.where(code[d : d + 1, :] == slot, 1.0, 0.0)
             parts.append(block)
-            weighted.append(block * shares[d, pl.ds(r, 1), :])
+            weighted.append(block * weight[d : d + 1, :])
         pick[r] = jnp.concatenate(parts, axis=0).astype(jnp.bfloat16)
         spread[r] = jnp.concatenate(weighted, axis=0).T.astype(jnp.bfloat16)
-        return carry
-
-    lax.fori_loop(0, Z, build, 0)
-    for copy in weight_copies():
-        copy.wait()
+
+    t_stage(jnp.int32(0))
+    build(0)
+
+    mixed_copy.wait_recv()
+    both = mixed[...].astype(jnp.float32) + mixed_in[...].astype(jnp.float32)
+    middle[...] = (tokens_ref[...].astype(jnp.float32) + both).astype(jnp.bfloat16)
+    values = middle[...].astype(jnp.float32)
+    factor = lax.rsqrt(jnp.mean(values * values, axis=-1, keepdims=True) + norm_eps)
+    normed[...] = (values * factor * gain_ref[...]).astype(jnp.bfloat16)
+
+    def own(c):
+        return pl.ds(pl.multiple_of(tp * H + c * W, W), W)
+
+    for c in range(nc):
+        gathered[0, c] = normed[:, own(c)]
+        z_stage(jnp.int32(0), c)
+
+    def shared_hidden():
+        for copy in shared_copies():
+            copy.wait()
+        acc = jnp.dot(normed[...], s_in[...], preferred_element_type=jnp.float32)
+        s_hidden[...] = (jax.nn.silu(acc[:, :SF]) * acc[:, SF:]).astype(jnp.bfloat16)
+
+    s_copy = send(s_part.at[other], s_part_in, s_sem.at[0], s_sem.at[1], partner)
+
+    def shared_partial():
+        for h in range(2):
+            for c in range(nc):
+                s_part[h, :, pl.ds(c * W, W)] = jnp.dot(
+                    s_hidden[...], s_out[:, pl.ds(h * H + c * W, W)], preferred_element_type=jnp.float32
+                ).astype(jnp.bfloat16)
+        s_copy.start()
 
     def x_copy(r, d):
         rows = pl.ds(d * R, R)
@@ -219,9 +286,9 @@
         for d in range(1, X):
             b_copy(r, d).start()
 
-    def of_pair(stage, k, way):
+    def of_pair(stage, k, way, least=0):
         if way == 0:
-            @pl.when((k >= 0) & (k <= half))
+            @pl.when((k >= least) & (k <= half))
             def _():
                 stage(k)
         else:
@@ -230,10 +297,30 @@
                 stage(Z - k)
 
     def step(i, carry):
+        @pl.when(i <= half)
+        def _():
+            t_stage(i)
+
         z_stage(i, 0)
+        of_pair(build, i, 0, 1)
+        of_pair(build, i, 1, 1)
         of_pair(select, i - 1, 0)
         of_pair(select, i - 1, 1)
         z_stage(i, 1)
+
+        @pl.when(i == 1)
+        def _():
+            shared_hidden()
+
+        @pl.when(i == 2)
+        def _():
+            shared_partial()
+
+        @pl.when(i == 3)
+        def _():
+            for copy in expert_copies():
+                copy.wait()
+
         of_pair(hand_over, i - 2, 0)
         of_pair(hand_over, i - 2, 1)
         of_pair(expert, i - 3, 0)
@@ -289,17 +376,25 @@
     lax.fori_loop(0, half, go_back, 0)
 
     back_wait(0)
+    s_copy.wait_recv()
     for c in range(nc):
-        mine = share_of(0, c) + base_ref[:, pl.ds(c * W, W)]
+        mine = share_of(0, c) + middle[:, own(c)].astype(jnp.float32)
+        mine = mine + s_part[tp, :, pl.ds(c * W, W)].astype(jnp.float32)
+        mine = mine + s_part_in[:, pl.ds(c * W, W)].astype(jnp.float32)
         r_copy(0, 1, c).wait_recv()
         r_copy(1, 1, c).wait_recv()
         mine = mine + sums_in[0, c].astype(jnp.float32) + sums_in[Z, c].astype(jnp.float32)
         out_ref[:, pl.ds(c * W, W)] = mine.astype(out_ref.dtype)
 
-    for k in range(1, Z):
-        table_copy(k).wait_send()
+    mixed_copy.wait_send()
+    s_copy.wait_send()
 
     def drain(k, carry):
+        for way in (0, 1):
+            @pl.when(k + 1 <= half - way)
+            def _():
+                t_copy(way, k).wait_send()
+
         for c in range(nc):
             for way in (0, 1):
                 limit = z_limit(way, c)
@@ -322,7 +417,7 @@
     lax.fori_loop(0, Z, drain_rows, 0)
 
 
-def moe(tokens, base, table, gate, up, down, top):
+def layer(active, tokens, gain, table, project, sgate, sup, sdown, gate, up, down, top):
     S, D = tokens.shape
     H = D // lax.axis_size("tp")
     X = ROW_RING
@@ -331,20 +426,29 @@
     W = H // nc
     R = 16
     F = gate.shape[2]
-    bf, f4 = jnp.bfloat16, jnp.float32
+    SF = sgate.shape[1]
+    bf = jnp.bfloat16
     dma = pltpu.SemaphoreType.DMA
     vm = pl.BlockSpec(memory_space=pltpu.VMEM)
     hb = pl.BlockSpec(memory_space=pl.ANY)
     return pl.pallas_call(
-        functools.partial(moe_kernel, (Z, X, S, H, R, nc, top)),
+        functools.partial(layer_kernel, (Z, X, S, H, R, nc, top)),
         out_shape=jax.ShapeDtypeStruct((S, H), bf),
-        in_specs=[vm, vm, vm, hb, hb, hb],
+        in_specs=[vm] * 4 + [hb] * 7,
         out_specs=vm,
         scratch_shapes=[
+            pltpu.VMEM(project.shape, bf),
+            pltpu.VMEM((S, D), bf),
+            pltpu.VMEM((S, D), bf),
+            pltpu.VMEM((S, D), bf),
+            pltpu.VMEM((S, D), bf),
+            pltpu.VMEM((D, 2 * SF), bf),
+            pltpu.VMEM((SF, D), bf),
+            pltpu.VMEM((S, SF), bf),
+            pltpu.VMEM((2, S, H), bf),
+            pltpu.VMEM((S, H), bf),
             pltpu.VMEM((Z, nc, S, W), bf),
-            pltpu.VMEM((Z, 16, LANES), f4),
-            pltpu.VMEM((X, Z, LANES), f4),
-            pltpu.VMEM((X, Z, LANES), f4),
+            pltpu.VMEM((Z, 16, LANES), bf),
             pltpu.VMEM((Z, X * R, LANES), bf),
             pltpu.VMEM((Z, LANES, X * R), bf),
             pltpu.VMEM((Z, nc, X * R, W), bf),
@@ -357,8 +461,10 @@
             pltpu.VMEM((Z, nc, X * R, W), bf),
             pltpu.VMEM((Z + 1, nc, S, W), bf),
             pltpu.VMEM((Z, nc, S, W), bf),
-            dma((3,)),
-            dma((Z,)),
+            dma((7,)),
+            dma((2,)),
+            dma((2,)),
+            dma((2, Z // 2)),
             dma((Z,)),
             dma((2, Z // 2, nc)),
             dma((Z, nc)),
@@ -374,67 +480,153 @@
             dma((Z + 1, nc)),
         ],
         compiler_params=pltpu.CompilerParams(
-            collective_id=0, has_side_effects=True, vmem_limit_bytes=48 * 1024 * 1024
+            collective_id=0, has_side_effects=True, vmem_limit_bytes=56 * 1024 * 1024
         ),
-        name="moe",
-    )(tokens, base, table, gate, up, down)
-
-
-def copy_for_each(value, axis):
-    peers = lax.axis_size(axis)
-    return lax.all_to_all(
-        jnp.broadcast_to(value[None], (peers, *value.shape)), axis, 0, 0, tiled=True
-    )
-
-
-def of_everyone(value, axis):
-    return copy_for_each(value, axis).astype(jnp.float32).sum(axis=0)
-
-
-def in_blocks(value, dim, peers):
-    before, after = (value.shape[:dim], value.shape[dim + 1 :])
-    return jnp.moveaxis(value.reshape(*before, peers, -1, *after), dim, 0)
-
-
-def summed_on_arrival(value, axis, dim):
-    tiles = in_blocks(value, dim, lax.axis_size(axis))
-    arrived = lax.all_to_all(tiles, axis, split_axis=0, concat_axis=0, tiled=True)
-    return arrived.astype(jnp.float32).sum(axis=0)
-
-
-def root_scale(activations, scale_gain):
-    values = activations.astype(jnp.float32)
-    factor = lax.rsqrt(jnp.mean(values * values, axis=-1, keepdims=True) + norm_eps)
-    return (values * factor * scale_gain).astype(jnp.bfloat16)
-
-
-def state_update(
-    drive_rows, prior_state, decay_rate, frequency, log_step, input_map, output_map, skip_gain
+        name="layer",
+    )(active, tokens, gain[None, :], table, project, sgate, sup, sdown, gate, up, down)
+
+
+def mixer_kernel(
+    tokens_ref,
+    prior_hbm,
+    gain_ref,
+    weight_hbm,
+    decay_ref,
+    freq_ref,
+    step_ref,
+    imap_ref,
+    omap_ref,
+    skip_ref,
+    active_ref,
+    state_hbm,
+    weight,
+    old,
+    fresh,
+    in_sem,
+    out_sem,
 ):
-    sequences = drive_rows.shape[0]
-    groups = decay_rate.shape[0]
-    driven = drive_rows.astype(jnp.float32).reshape(sequences, groups, -1)
-    step_size = jnp.exp(log_step)[:, None]
-    real_rate = -decay_rate
+    S, D = tokens_ref.shape
+    width = weight.shape[1]
+    groups, entries = decay_ref.shape
+    members = width // groups
+    f4, bf = jnp.float32, jnp.bfloat16
+    lane_groups = LANES // entries
+    block = LANES // members
+    cols = block * entries
+
+    def weight_copy():
+        return pltpu.make_async_copy(weight_hbm, weight, in_sem.at[0])
+
+    def old_copy(part):
+        return pltpu.make_async_copy(prior_hbm.at[part], old.at[part], in_sem.at[1 + part])
+
+    def state_copy(part, q):
+        lanes = pl.ds(q * cols, cols)
+        return pltpu.make_async_copy(fresh.at[part, :, lanes], state_hbm.at[part, :, lanes], out_sem.at[part, q])
+
+    weight_copy().start()
+    old_copy(0).start()
+    old_copy(1).start()
+
+    eye = lax.broadcasted_iota(jnp.int32, (groups, groups), 0) == lax.broadcasted_iota(jnp.int32, (groups, groups), 1)
+    log_column = jnp.sum(jnp.where(eye, step_ref[...], 0.0), axis=1, keepdims=True)
+    step_size = jnp.exp(log_column)
+    real_rate = -decay_ref[...]
+    frequency = freq_ref[...]
     magnitude = jnp.exp(real_rate * step_size)
     turn_real = magnitude * jnp.cos(frequency * step_size)
     turn_imag = magnitude * jnp.sin(frequency * step_size)
     denominator = real_rate * real_rate + frequency * frequency
     hold_real = ((turn_real - 1.0) * real_rate + turn_imag * frequency) / denominator
     hold_imag = (turn_imag * real_rate - (turn_real - 1.0) * frequency) / denominator
-    push_real = jnp.einsum("sgh,gph->sgp", driven, input_map[0])
-    push_imag = jnp.einsum("sgh,gph->sgp", driven, input_map[1])
-    enter_real = push_real * hold_real - push_imag * hold_imag
-    enter_imag = push_real * hold_imag + push_imag * hold_real
-    old_real = prior_state[0].reshape(sequences, groups, -1)
-    old_imag = prior_state[1].reshape(sequences, groups, -1)
-    fresh_real = turn_real * old_real - turn_imag * old_imag + enter_real
-    fresh_imag = turn_real * old_imag + turn_imag * old_real + enter_imag
-    readout = jnp.einsum("ghp,sgp->sgh", output_map[0], fresh_real)
-    readout = readout - jnp.einsum("ghp,sgp->sgh", output_map[1], fresh_imag)
-    readout = readout.reshape(sequences, -1) + skip_gain * drive_rows.astype(jnp.float32)
-    fresh = jnp.stack([fresh_real.reshape(sequences, -1), fresh_imag.reshape(sequences, -1)])
-    return (readout, fresh)
+    doubled = [jnp.concatenate([v] * lane_groups, axis=1) for v in (turn_real, turn_imag, hold_real, hold_imag)]
+    row_group = lax.broadcasted_iota(jnp.int32, (groups, LANES), 0)
+    lane_group = lax.broadcasted_iota(jnp.int32, (groups, LANES), 1) // entries
+
+    values = tokens_ref[...].astype(f4)
+    factor = lax.rsqrt(jnp.mean(values * values, axis=-1, keepdims=True) + norm_eps)
+    normed = (values * factor * gain_ref[...]).astype(bf)
+    weight_copy().wait()
+    drive = jnp.dot(normed, weight[...], preferred_element_type=f4).astype(bf)
+    old_copy(0).wait()
+    old_copy(1).wait()
+
+    in_row = lax.broadcasted_iota(jnp.int32, (LANES, LANES), 0) // members
+    in_lane = lax.broadcasted_iota(jnp.int32, (LANES, LANES), 1) // entries
+    out_row = lax.broadcasted_iota(jnp.int32, (LANES, 2 * LANES), 0) // members
+    out_lane = lax.broadcasted_iota(jnp.int32, (LANES, 2 * LANES), 1) // entries
+
+    for q in range(width // LANES):
+        channels = slice(q * LANES, (q + 1) * LANES)
+        mine = drive[:, channels]
+        maps = [jnp.concatenate([imap_ref[part, channels, :]] * lane_groups, axis=1) for part in range(2)]
+        outs = [jnp.concatenate([omap_ref[part, channels, :]] * (2 * lane_groups), axis=1) for part in range(2)]
+        readout = mine.astype(f4) * skip_ref[:, channels]
+        for m in range(cols // LANES):
+            mask = in_row == in_lane + m * lane_groups
+            both = jnp.concatenate([jnp.where(mask, v, 0.0) for v in maps], axis=1).astype(bf)
+            push = jnp.dot(mine, both, preferred_element_type=f4)
+            push_real, push_imag = push[:, :LANES], push[:, LANES:]
+            first = q * block + m * lane_groups
+            tr, ti, hr, hi = [
+                jnp.sum(jnp.where(row_group == lane_group + first, v, 0.0), axis=0, keepdims=True) for v in doubled
+            ]
+            at = slice(q * cols + m * LANES, q * cols + (m + 1) * LANES)
+            old_real, old_imag = old[0, :, at], old[1, :, at]
+            fresh[0, :, at] = tr * old_real - ti * old_imag + (push_real * hr - push_imag * hi)
+            fresh[1, :, at] = tr * old_imag + ti * old_real + (push_real * hi + push_imag * hr)
+        state_copy(0, q).start()
+        state_copy(1, q).start()
+        for h in range(cols // (2 * LANES)):
+            at = slice(q * cols + h * 2 * LANES, q * cols + (h + 1) * 2 * LANES)
+            mask = out_row == out_lane + h * 2 * lane_groups
+            for part in range(2):
+                spread_out = jnp.where(mask, outs[part] if part == 0 else -outs[part], 0.0).astype(bf)
+                readout = readout + lax.dot_general(
+                    fresh[part, :, at].astype(bf), spread_out, (((1,), (1,)), ((), ())), preferred_element_type=f4
+                )
+        active_ref[:, channels] = jax.nn.gelu(readout).astype(bf)
+    for q in range(width // LANES):
+        for part in range(2):
+            state_copy(part, q).wait()
+
+
+def mixer(tokens, prior, gain, weight, decay, freq, log_step, imap, omap, skip):
+    S, D = tokens.shape
+    width = weight.shape[1]
+    vm = pl.BlockSpec(memory_space=pltpu.VMEM)
+    hb = pl.BlockSpec(memory_space=pl.ANY)
+    dma = pltpu.SemaphoreType.DMA
+    by_channel = (2, width, imap.shape[2])
+    return pl.pallas_call(
+        mixer_kernel,
+        out_shape=(
+            jax.ShapeDtypeStruct((S, width), jnp.bfloat16),
+            jax.ShapeDtypeStruct(prior.shape, jnp.float32),
+        ),
+        in_specs=[vm, hb, vm, hb, vm, vm, vm, vm, vm, vm],
+        out_specs=(vm, hb),
+        scratch_shapes=[
+            pltpu.VMEM(weight.shape, weight.dtype),
+            pltpu.VMEM(prior.shape, jnp.float32),
+            pltpu.VMEM(prior.shape, jnp.float32),
+            dma((3,)),
+            dma((2, width // LANES)),
+        ],
+        compiler_params=pltpu.CompilerParams(vmem_limit_bytes=32 * 1024 * 1024),
+        name="mixer",
+    )(
+        tokens,
+        prior,
+        gain[None, :],
+        weight,
+        decay,
+        freq,
+        log_step[None, :],
+        jnp.swapaxes(imap, 2, 3).reshape(by_channel),
+        omap.reshape(by_channel),
+        skip[None, :],
+    )
 
 
 def body(
@@ -459,24 +651,9 @@
     routes,
     route_weights,
 ):
-    normed = root_scale(tokens, mix_gain)
-    drive_rows = jnp.dot(normed, in_weight, preferred_element_type=jnp.float32).astype(jnp.bfloat16)
-    readout, new_state = state_update(
-        drive_rows, prior_state, decay_rate, frequency, log_step, input_map, output_map, skip_gain
+    activated, new_state = mixer(
+        tokens, prior_state, mix_gain, in_weight, decay_rate, frequency, log_step, input_map, output_map, skip_gain
     )
-    activated = jax.nn.gelu(readout).astype(jnp.bfloat16)
-    partial_value = jnp.dot(activated, out_weight, preferred_element_type=jnp.float32)
-    mixer_out = of_everyone(partial_value.astype(jnp.bfloat16), "tp").astype(jnp.float32)
-    middle = (tokens.astype(jnp.float32) + mixer_out).astype(jnp.bfloat16)
-    second_normed = root_scale(middle, channel_gain)
-    shared_gval = jnp.dot(second_normed, shared_gate, preferred_element_type=jnp.float32)
-    shared_uval = jnp.dot(second_normed, shared_up, preferred_element_type=jnp.float32)
-    shared_hidden = (jax.nn.silu(shared_gval) * shared_uval).astype(jnp.bfloat16)
-    shared_piece = jnp.dot(shared_hidden, shared_down, preferred_element_type=jnp.float32)
-    shared_out = summed_on_arrival(shared_piece.astype(jnp.bfloat16), "tp", 1)
-    half_cols = middle.shape[1] // lax.axis_size("tp")
-    own_middle = lax.dynamic_slice_in_dim(middle, lax.axis_index("tp") * half_cols, half_cols, 1)
-    base = own_middle.astype(jnp.float32) + shared_out
     seq_rows, top_count = routes.shape
     pad = ((0, 8 - top_count), (0, LANES - seq_rows))
     table = jnp.concatenate(
@@ -485,8 +662,21 @@
             jnp.pad(route_weights.T, pad),
         ],
         axis=0,
+    ).astype(jnp.bfloat16)
+    layer_out = layer(
+        activated,
+        tokens,
+        channel_gain,
+        table,
+        out_weight,
+        shared_gate,
+        shared_up,
+        shared_down,
+        expert_gate,
+        expert_up,
+        expert_down,
+        top_count,
     )
-    layer_out = moe(second_normed, base, table, expert_gate, expert_up, expert_down, top_count)
     return (layer_out, new_state)
 
 

time: 181 us -> 144 us (0.80)
  matrix products: 11.4 us -> 0 us
  local copies, waits for them, and re-layouts: 17.6 us -> 11.8 us
  Pallas kernels: 134 us -> 129 us
  other arithmetic: 6.67 us -> 1.97 us
  blocking collectives: 4.51 us -> 0 us
  starting transfers between devices: 4.2 us -> 0 us
    dot_general x8 -> x0, matrix products: 11.4 us -> none  [the longest x1 3.04 us: state_update(): push_imag = jnp.einsum('sgh,gph->sgp', driven, input_map[1])]
    unnamed x43 -> x23, local copies, waits for them, and re-layouts: 4.19 us -> 11.8 us
    slice x3 -> x0, local copies, waits for them, and re-layouts: 6.61 us -> none  [the longest x2 4.15 us: state_update(): old_real = prior_state[0].reshape(sequences, groups, -1)]
    pallas_call x1 -> x2, Pallas kernels: 134 us -> 129 us  [the longest x1 126 us: layer(): pl.pallas_call(functools.partial(layer_kernel, (Z, X, S, H, R, nc, top)),...]
    all_to_all x1 -> x0, blocking collectives: 4.51 us -> none  [copy_for_each(): lax.all_to_all(jnp.broadcast_to(value[None], (peers, *value.shape)), axis...]
    all_to_all x1 -> x0, starting transfers between devices: 4.2 us -> none  [summed_on_arrival(): lax.all_to_all(tiles, axis, split_axis=0, concat_axis=0, tiled=True)]
    another operation x2 -> x0, local copies, waits for them, and re-layouts: 3.81 us -> none  [state_update(): jnp.stack([fresh_real.reshape(sequences, -1), fresh_imag.reshape(sequence...]
    reduce_sum x4 -> x0, other arithmetic: 2.7 us -> none  [the longest x2 1.39 us: root_scale(): jnp.mean(values * values, axis=-1, keepdims=True) + norm_eps]
  transfers between devices with their start and end apart: 1 -> 0, of which waited for: 1 -> 0; matrix products, arithmetic and copies ran while one was open for 0% -> 0% of each run, Pallas kernels for 0% -> 0%
where the time goes in v2:
time: 144 us; the launch traced here: 143 us
  Pallas kernels  129 us (90%)
  local copies, waits for them, and re-layouts  11.8 us (8%)
  other arithmetic  1.97 us (1%)
    pallas_call x1, Pallas kernels, layer(): pl.pallas_call(functools.partial(layer_kernel, (Z, X, S, H, R, nc, top)),...  126 us
    unnamed x23, local copies, waits for them, and re-layouts  11.8 us

profile of v2, /device:TPU:40, one launch (start us, length us, event | category | flops | bytes accessed | tf_op | source)
XLA Modules:
  0.0 143.0 jit_solution(6410246002081684183)
XLA Ops:
  0.6 0.7 fusion.3
  1.3 0.7 convert_bitcast_fusion
  2.0 0.6 fusion.2.table_ref
  2.6 0.0 copy-start
  2.6 1.6 %copy-done = bf16[2048,512]{1,0:T(8,128)(2,1)S(1)} copy-done((bf16[2048,512]{1,0:T(8,128)(2,1)S(1)}, bf16[2048,512]{1,0:T(8,128)(2,1)}, u32[]{:S(2)}) %copy-start) | copy-done | bytes 2097176
  4.2 0.0 copy-start.1
  4.2 1.0 copy-done.1
  5.2 0.0 copy-start.2
  5.2 1.4 copy-done.2
  6.6 0.0 copy-start.3
  6.6 1.0 copy-done.3
  7.6 0.0 copy-start.4
  7.6 1.0 copy-done.4
  8.7 0.0 copy-start.6
  8.7 0.7 copy-done.6
  9.4 0.0 copy-start.7
  9.4 0.7 copy-done.7
  10.1 0.0 copy-start.8
  10.1 0.7 copy-done.8
  10.8 0.0 copy-start.9
  10.8 0.7 copy-done.9
  11.5 0.0 copy-start.10
  11.5 0.7 copy-done.10
  12.2 2.7 %mixer.1 = (bf16[96,512]{1,0:T(8,128)(2,1)S(1)}, f32[2,96,2048]{2,1,0:T(8,128)}) custom-call(bf16[96,2048]{1,0:T(8,128)(2,1)S(1)} %copy-done.1, f32[2,96,2048]{2,1,0:T(8,128)S(1)} %copy-done.2, f32[1,2048]{1,0:T(1,128)S(1)} %bitcast.14, bf16[2048,512]{1,0:T(8,128)(2,1)S(1)} %copy-done, f32[32,64]{1,0:T(8,128)S(1)} %copy-done.6, f32[32,64]{1,0:T(8,128)S(1)} %copy-done.7, ...), custom_call_target="tpu_custom_call" | custom-call | tf_op jit(solution)/shard_map/mixer/pallas_call | solution.py:601
  14.9 0.0 copy-start.5
  14.9 0.6 copy-done.5
  15.5 125.9 %layer.1 = bf16[96,1024]{1,0:T(8,128)(2,1)} custom-call(bf16[96,512]{1,0:T(8,128)(2,1)} %copy-done.5, bf16[96,2048]{1,0:T(8,128)(2,1)} %tokens_ref.3, f32[1,2048]{1,0:T(1,128)} %bitcast.17, bf16[16,128]{1,0:T(8,128)(2,1)} %fusion.2.table_ref, bf16[512,2048]{1,0:T(8,128)(2,1)} %project_hbm.1, bf16[2048,256]{1,0:T(8,128)(2,1)} %sgate_hbm.1, ...), custom_call_target="tpu_custom_call" | custom-call | tf_op jit(solution)/shard_map/layer/pallas_call | solution.py:434
  141.4 1.6 %copy.23 = bf16[96,1024]{1,0:T(8,128)(2,1)} copy(bf16[96,1024]{1,0:T(8,128)(2,1)} %layer.1) | data formatting | bytes 393216
Async XLA Ops:
  2.6 1.6 %copy-start = (bf16[2048,512]{1,0:T(8,128)(2,1)S(1)}, bf16[2048,512]{1,0:T(8,128)(2,1)}, u32[]{:S(2)}) copy-start(bf16[2048,512]{1,0:T(8,128)(2,1)} %weight_hbm.1) | copy-start | bytes 6291460
  4.2 1.0 copy-start.1
  5.2 1.4 copy-start.2
  6.6 1.0 copy-start.3
  7.6 1.0 copy-start.4
  8.7 0.7 copy-start.6
  9.4 0.7 copy-start.7
  10.1 0.7 copy-start.8
  10.8 0.7 copy-start.9
  11.5 0.7 copy-start.10
  14.9 0.6 copy-start.5

commit v3 on v2

--- a/solution.py
+++ b/solution.py
@@ -12,15 +12,16 @@
 ROW_RING = 4
 CHUNKS = 4
 LANES = 128
+VMEM_ALL = 63 * 1024 * 1024
 
 
 def layer_kernel(
     cfg,
-    active_ref,
-    tokens_ref,
-    gain_ref,
-    table_ref,
-    project_hbm,
+    mixed_hbm,
+    tokens_hbm,
+    gain_hbm,
+    routes_hbm,
+    shares_hbm,
     sgate_hbm,
     sup_hbm,
     sdown_hbm,
@@ -28,7 +29,11 @@
     up_hbm,
     down_hbm,
     out_ref,
-    project,
+    tokens_ref,
+    gain_ref,
+    routes_ref,
+    shares_ref,
+    table,
     mixed,
     mixed_in,
     middle,
@@ -94,9 +99,6 @@
             device_id=device, device_id_type=MESH,
         )
 
-    def project_copy():
-        return pltpu.make_async_copy(project_hbm, project, w_sem.at[0])
-
     def shared_copies():
         return (
             pltpu.make_async_copy(sgate_hbm, s_in.at[:, pl.ds(0, SF)], w_sem.at[1]),
@@ -111,21 +113,33 @@
             pltpu.make_async_copy(down_hbm.at[0], w_out, w_sem.at[6]),
         )
 
-    project_copy().start()
+    small = [
+        pltpu.make_async_copy(src, dst, w_sem.at[7 + i])
+        for i, (src, dst) in enumerate(
+            (
+                (mixed_hbm, mixed),
+                (routes_hbm, routes_ref),
+                (shares_hbm, shares_ref),
+                (tokens_hbm, tokens_ref),
+                (gain_hbm, gain_ref),
+            )
+        )
+    ]
+    for copy in small:
+        copy.start()
 
     barrier = pltpu.get_barrier_semaphore()
     for device in (at_z(1), at_z(-1), *[at_x(d) for d in range(1, X)], partner):
         pl.semaphore_signal(barrier, inc=1, device_id=device, device_id_type=MESH)
 
-    tables[0] = table_ref[...]
-    project_copy().wait()
+    table[...] = jnp.where(lax.broadcasted_iota(jnp.int32, (16, LANES), 0) < 8, -1.0, 0.0)
+    for copy in small[:3]:
+        copy.wait()
+    table[pl.ds(0, top), pl.ds(0, S)] = routes_ref[...].astype(jnp.float32)
+    table[pl.ds(8, top), pl.ds(0, S)] = shares_ref[...]
+    tables[0] = table[...].astype(jnp.bfloat16)
     for copy in (*shared_copies(), *expert_copies()):
         copy.start()
-    active = active_ref[...]
-    for h in range(2 * nc):
-        cols = slice(h * W, (h + 1) * W)
-        mixed[:, cols] = jnp.dot(active, project[:, cols], preferred_element_type=jnp.float32).astype(jnp.bfloat16)
-
     pl.semaphore_wait(barrier, X + 2)
 
     mixed_copy = send(mixed, mixed_in, m_sem.at[0], m_sem.at[1], partner)
@@ -201,6 +215,8 @@
     t_stage(jnp.int32(0))
     build(0)
 
+    for copy in small[3:]:
+        copy.wait()
     mixed_copy.wait_recv()
     both = mixed[...].astype(jnp.float32) + mixed_in[...].astype(jnp.float32)
     middle[...] = (tokens_ref[...].astype(jnp.float32) + both).astype(jnp.bfloat16)
@@ -283,6 +299,8 @@
             y = (partial[r, tp, c].astype(jnp.float32) + partner_part[r, c].astype(jnp.float32)).astype(jnp.bfloat16)
             back[r, c, pl.ds(0, R), :] = y[:R]
             total[r, c] = y
+
+    def hand_back(r):
         for d in range(1, X):
             b_copy(r, d).start()
 
@@ -329,6 +347,12 @@
         of_pair(join, i - 4, 0)
         z_stage(i, 3)
         of_pair(join, i - 4, 1)
+
+        @pl.when(i - 4 >= half - 1)
+        def _():
+            of_pair(hand_back, i - 4, 0)
+            of_pair(hand_back, i - 4, 1)
+
         return carry
 
     lax.fori_loop(1, half + 5, step, 0)
@@ -346,6 +370,8 @@
 
     def go_back(i, carry):
         k = half - i
+        of_pair(hand_back, k - 2, 0)
+        of_pair(hand_back, k - 2, 1)
         back_wait(k)
 
         @pl.when(k < half)
@@ -417,7 +443,8 @@
     lax.fori_loop(0, Z, drain_rows, 0)
 
 
-def layer(active, tokens, gain, table, project, sgate, sup, sdown, gate, up, down, top):
+def layer(mixed, tokens, gain, routes, shares, sgate, sup, sdown, gate, up, down):
+    top = routes.shape[1]
     S, D = tokens.shape
     H = D // lax.axis_size("tp")
     X = ROW_RING
@@ -434,10 +461,14 @@
     return pl.pallas_call(
         functools.partial(layer_kernel, (Z, X, S, H, R, nc, top)),
         out_shape=jax.ShapeDtypeStruct((S, H), bf),
-        in_specs=[vm] * 4 + [hb] * 7,
+        in_specs=[hb] * 11,
         out_specs=vm,
         scratch_shapes=[
-            pltpu.VMEM(project.shape, bf),
+            pltpu.VMEM((S, D), bf),
+            pltpu.VMEM((1, D), jnp.float32),
+            pltpu.VMEM((top, S), jnp.int32),
+            pltpu.VMEM((top, S), jnp.float32),
+            pltpu.VMEM((16, LANES), jnp.float32),
             pltpu.VMEM((S, D), bf),
             pltpu.VMEM((S, D), bf),
             pltpu.VMEM((S, D), bf),
@@ -461,7 +492,7 @@
             pltpu.VMEM((Z, nc, X * R, W), bf),
             pltpu.VMEM((Z + 1, nc, S, W), bf),
             pltpu.VMEM((Z, nc, S, W), bf),
-            dma((7,)),
+            dma((12,)),
             dma((2,)),
             dma((2,)),
             dma((2, Z // 2)),
@@ -480,30 +511,43 @@
             dma((Z + 1, nc)),
         ],
         compiler_params=pltpu.CompilerParams(
-            collective_id=0, has_side_effects=True, vmem_limit_bytes=56 * 1024 * 1024
+            collective_id=0, has_side_effects=True, vmem_limit_bytes=VMEM_ALL
         ),
         name="layer",
-    )(active, tokens, gain[None, :], table, project, sgate, sup, sdown, gate, up, down)
+    )(mixed, tokens, gain[None, :], routes.T, shares.T, sgate, sup, sdown, gate, up, down)
 
 
 def mixer_kernel(
+    tokens_hbm,
+    prior_hbm,
+    gain_hbm,
+    weight_hbm,
+    decay_hbm,
+    freq_hbm,
+    step_hbm,
+    imap_hbm,
+    omap_hbm,
+    skip_hbm,
+    project_hbm,
+    mixed_hbm,
+    state_hbm,
     tokens_ref,
-    prior_hbm,
+    old,
     gain_ref,
-    weight_hbm,
+    weight,
     decay_ref,
     freq_ref,
     step_ref,
     imap_ref,
     omap_ref,
     skip_ref,
+    project,
     active_ref,
-    state_hbm,
-    weight,
-    old,
+    mixed,
     fresh,
     in_sem,
     out_sem,
+    mixed_sem,
 ):
     S, D = tokens_ref.shape
     width = weight.shape[1]
@@ -514,19 +558,31 @@
     block = LANES // members
     cols = block * entries
 
-    def weight_copy():
-        return pltpu.make_async_copy(weight_hbm, weight, in_sem.at[0])
-
-    def old_copy(part):
-        return pltpu.make_async_copy(prior_hbm.at[part], old.at[part], in_sem.at[1 + part])
+    fetched = {}
+    for i, (name, src, dst) in enumerate(
+        (
+            ("tokens", tokens_hbm, tokens_ref),
+            ("gain", gain_hbm, gain_ref),
+            ("step", step_hbm, step_ref),
+            ("decay", decay_hbm, decay_ref),
+            ("freq", freq_hbm, freq_ref),
+            ("weight", weight_hbm, weight),
+            ("imap", imap_hbm, imap_ref),
+            ("old", prior_hbm, old),
+            ("skip", skip_hbm, skip_ref),
+            ("omap", omap_hbm, omap_ref),
+            ("project", project_hbm, project),
+        )
+    ):
+        fetched[name] = pltpu.make_async_copy(src, dst, in_sem.at[i])
+        fetched[name].start()
 
     def state_copy(part, q):
         lanes = pl.ds(q * cols, cols)
         return pltpu.make_async_copy(fresh.at[part, :, lanes], state_hbm.at[part, :, lanes], out_sem.at[part, q])
 
-    weight_copy().start()
-    old_copy(0).start()
-    old_copy(1).start()
+    for name in ("step", "decay", "freq"):
+        fetched[name].wait()
 
     eye = lax.broadcasted_iota(jnp.int32, (groups, groups), 0) == lax.broadcasted_iota(jnp.int32, (groups, groups), 1)
     log_column = jnp.sum(jnp.where(eye, step_ref[...], 0.0), axis=1, keepdims=True)
@@ -543,13 +599,15 @@
     row_group = lax.broadcasted_iota(jnp.int32, (groups, LANES), 0)
     lane_group = lax.broadcasted_iota(jnp.int32, (groups, LANES), 1) // entries
 
+    fetched["tokens"].wait()
+    fetched["gain"].wait()
     values = tokens_ref[...].astype(f4)
     factor = lax.rsqrt(jnp.mean(values * values, axis=-1, keepdims=True) + norm_eps)
     normed = (values * factor * gain_ref[...]).astype(bf)
-    weight_copy().wait()
+    fetched["weight"].wait()
     drive = jnp.dot(normed, weight[...], preferred_element_type=f4).astype(bf)
-    old_copy(0).wait()
-    old_copy(1).wait()
+    for name in ("imap", "old", "skip", "omap"):
+        fetched[name].wait()
 
     in_row = lax.broadcasted_iota(jnp.int32, (LANES, LANES), 0) // members
     in_lane = lax.broadcasted_iota(jnp.int32, (LANES, LANES), 1) // entries
@@ -586,34 +644,56 @@
                     fresh[part, :, at].astype(bf), spread_out, (((1,), (1,)), ((), ())), preferred_element_type=f4
                 )
         active_ref[:, channels] = jax.nn.gelu(readout).astype(bf)
+    fetched["project"].wait()
+    quarter = D // 4
+    sent = []
+    for h in range(4):
+        at = slice(h * quarter, (h + 1) * quarter)
+        mixed[:, at] = jnp.dot(active_ref[...], project[:, at], preferred_element_type=f4).astype(bf)
+        sent.append(pltpu.make_async_copy(mixed.at[:, at], mixed_hbm.at[:, at], mixed_sem.at[h]))
+        sent[-1].start()
+    for copy in sent:
+        copy.wait()
     for q in range(width // LANES):
         for part in range(2):
             state_copy(part, q).wait()
 
 
-def mixer(tokens, prior, gain, weight, decay, freq, log_step, imap, omap, skip):
+def mixer(tokens, prior, gain, weight, decay, freq, log_step, imap, omap, skip, project):
     S, D = tokens.shape
     width = weight.shape[1]
-    vm = pl.BlockSpec(memory_space=pltpu.VMEM)
+    f4 = jnp.float32
     hb = pl.BlockSpec(memory_space=pl.ANY)
     dma = pltpu.SemaphoreType.DMA
     by_channel = (2, width, imap.shape[2])
     return pl.pallas_call(
         mixer_kernel,
         out_shape=(
-            jax.ShapeDtypeStruct((S, width), jnp.bfloat16),
+            jax.ShapeDtypeStruct((S, D), jnp.bfloat16),
             jax.ShapeDtypeStruct(prior.shape, jnp.float32),
         ),
-        in_specs=[vm, hb, vm, hb, vm, vm, vm, vm, vm, vm],
-        out_specs=(vm, hb),
+        in_specs=[hb] * 11,
+        out_specs=(hb, hb),
         scratch_shapes=[
+            pltpu.VMEM((S, D), tokens.dtype),
+            pltpu.VMEM(prior.shape, f4),
+            pltpu.VMEM((1, D), f4),
             pltpu.VMEM(weight.shape, weight.dtype),
-            pltpu.VMEM(prior.shape, jnp.float32),
-            pltpu.VMEM(prior.shape, jnp.float32),
-            dma((3,)),
+            pltpu.VMEM(decay.shape, f4),
+            pltpu.VMEM(freq.shape, f4),
+            pltpu.VMEM((1, log_step.shape[0]), f4),
+            pltpu.VMEM(by_channel, f4),
+            pltpu.VMEM(by_channel, f4),
+            pltpu.VMEM((1, width), f4),
+            pltpu.VMEM(project.shape, project.dtype),
+            pltpu.VMEM((S, width), tokens.dtype),
+            pltpu.VMEM((S, D), tokens.dtype),
+            pltpu.VMEM(prior.shape, f4),
+            dma((11,)),
             dma((2, width // LANES)),
+            dma((4,)),
         ],
-        compiler_params=pltpu.CompilerParams(vmem_limit_bytes=32 * 1024 * 1024),
+        compiler_params=pltpu.CompilerParams(vmem_limit_bytes=VMEM_ALL),
         name="mixer",
     )(
         tokens,
@@ -626,6 +706,7 @@
         jnp.swapaxes(imap, 2, 3).reshape(by_channel),
         omap.reshape(by_channel),
         skip[None, :],
+        project,
     )
 
 
@@ -651,31 +732,31 @@
     routes,
     route_weights,
 ):
-    activated, new_state = mixer(
-        tokens, prior_state, mix_gain, in_weight, decay_rate, frequency, log_step, input_map, output_map, skip_gain
+    mixed, new_state = mixer(
+        tokens,
+        prior_state,
+        mix_gain,
+        in_weight,
+        decay_rate,
+        frequency,
+        log_step,
+        input_map,
+        output_map,
+        skip_gain,
+        out_weight,
     )
-    seq_rows, top_count = routes.shape
-    pad = ((0, 8 - top_count), (0, LANES - seq_rows))
-    table = jnp.concatenate(
-        [
-            jnp.pad(routes.T.astype(jnp.float32), pad, constant_values=-1.0),
-            jnp.pad(route_weights.T, pad),
-        ],
-        axis=0,
-    ).astype(jnp.bfloat16)
     layer_out = layer(
-        activated,
+        mixed,
         tokens,
         channel_gain,
-        table,
-        out_weight,
+        routes,
+        route_weights,
         shared_gate,
         shared_up,
         shared_down,
         expert_gate,
         expert_up,
         expert_down,
-        top_count,
     )
     return (layer_out, new_state)
 

time: 144 us -> 126 us (0.88)
  local copies, waits for them, and re-layouts: 11.8 us -> 1.62 us
  Pallas kernels: 129 us -> 124 us
  other arithmetic: 1.97 us -> 0 us
    unnamed x23 -> x1, local copies, waits for them, and re-layouts: 11.8 us -> 1.62 us
    pallas_call x1, Pallas kernels: 126 us -> 119 us  [layer(): pl.pallas_call(functools.partial(layer_kernel, (Z, X, S, H, R, nc, top)),...]
    pallas_call x1, Pallas kernels: 2.72 us -> 4.92 us  [mixer(): pl.pallas_call(mixer_kernel, out_shape=(jax.ShapeDtypeStruct((S, D), jnp....]
where the time goes in v3:
time: 126 us
  Pallas kernels  124 us (98%)
  local copies, waits for them, and re-layouts  1.62 us (1%)
    pallas_call x1, Pallas kernels, layer(): pl.pallas_call(functools.partial(layer_kernel, (Z, X, S, H, R, nc, top)),...  119 us
    pallas_call x1, Pallas kernels, mixer(): pl.pallas_call(mixer_kernel, out_shape=(jax.ShapeDtypeStruct((S, D), jnp....  4.92 us

profile of v3, /device:TPU:40, one launch (start us, length us, event | category | flops | bytes accessed | tf_op | source)
XLA Modules:
  0.0 125.9 jit_solution(14964570243753736469)
XLA Ops:
  0.6 4.9 %mixer.1 = (bf16[96,2048]{1,0:T(8,128)(2,1)}, f32[2,96,2048]{2,1,0:T(8,128)}) custom-call(bf16[96,2048]{1,0:T(8,128)(2,1)} %tokens_hbm.3, f32[2,96,2048]{2,1,0:T(8,128)} %prior_hbm.1, f32[1,2048]{1,0:T(1,128)} %bitcast.12, bf16[2048,512]{1,0:T(8,128)(2,1)} %weight_hbm.1, f32[32,64]{1,0:T(8,128)} %decay_hbm.1, f32[32,64]{1,0:T(8,128)} %freq_hbm.1, ...), custom_call_target="tpu_custom_call" | custom-call | tf_op jit(solution)/shard_map/mixer/pallas_call | solution.py:669
  5.6 118.7 %layer.1 = bf16[96,1024]{1,0:T(8,128)(2,1)} custom-call(bf16[96,2048]{1,0:T(8,128)(2,1)} %get-tuple-element.4.mixed_hbm, bf16[96,2048]{1,0:T(8,128)(2,1)} %tokens_hbm.3, f32[1,2048]{1,0:T(1,128)} %bitcast.13, s32[6,96]{1,0:T(8,128)} %bitcast.14, f32[6,96]{1,0:T(8,128)} %bitcast.15, bf16[2048,256]{1,0:T(8,128)(2,1)} %sgate_hbm.1, bf16[2048,256]{1,0:T(8,128)(2,1)} %sup_hbm.1, ...), custom_call_target="tpu_custom_call" | custom-call | tf_op jit(solution)/shard_map/layer/pallas_call | solution.py:461
  124.3 1.6 %copy.23 = bf16[96,1024]{1,0:T(8,128)(2,1)} copy(bf16[96,1024]{1,0:T(8,128)(2,1)} %layer.1) | data formatting | bytes 393216

commit v4 on v3

--- a/solution.py
+++ b/solution.py
@@ -57,6 +57,10 @@
     back,
     sums_in,
     sums_out,
+    far_pick,
+    far_spread,
+    far_staged,
+    far_back,
     w_sem,
     m_sem,
     s_sem,
@@ -74,6 +78,9 @@
     b_recv,
     r_send,
     r_recv,
+    f_send,
+    f_recv,
+    g_send,
 ):
     Z, X, S, H, R, nc, top = cfg
     W = H // nc
@@ -91,7 +98,11 @@
     def at_x(offset):
         return {"ep": z * X + lax.rem(x + offset + X, X)}
 
+    def at_far(dz, dx):
+        return {"ep": lax.rem(z + dz + Z, Z) * X + lax.rem(x + dx + X, X)}
+
     partner = {"tp": other}
+    hc = nc // 2
 
     def send(src, dst, s_sem, r_sem, device):
         return pltpu.make_async_remote_copy(
@@ -129,7 +140,7 @@
         copy.start()
 
     barrier = pltpu.get_barrier_semaphore()
-    for device in (at_z(1), at_z(-1), *[at_x(d) for d in range(1, X)], partner):
+    for device in (*[at_far(s, d) for s in (1, -1) for d in range(X)], *[at_x(d) for d in range(1, X)], partner):
         pl.semaphore_signal(barrier, inc=1, device_id=device, device_id_type=MESH)
 
     table[...] = jnp.where(lax.broadcasted_iota(jnp.int32, (16, LANES), 0) < 8, -1.0, 0.0)
@@ -140,7 +151,7 @@
     tables[0] = table[...].astype(jnp.bfloat16)
     for copy in (*shared_copies(), *expert_copies()):
         copy.start()
-    pl.semaphore_wait(barrier, X + 2)
+    pl.semaphore_wait(barrier, 3 * X)
 
     mixed_copy = send(mixed, mixed_in, m_sem.at[0], m_sem.at[1], partner)
     mixed_copy.start()
@@ -153,7 +164,7 @@
 
     def t_stage(k):
         for way in (0, 1):
-            limit = half - way
+            limit = half - 1
 
             @pl.when((k >= 1) & (k <= limit))
             def _():
@@ -169,13 +180,9 @@
         r = lax.rem(Z - k, Z)
         return send(gathered.at[r, c], gathered.at[Z - k - 1, c], z_send.at[1, k, c], z_recv.at[Z - k - 1, c], at_z(-1))
 
-    def z_limit(way, c):
-        mine = (c < nc // 2) if way == 0 else (c >= nc // 2)
-        return half if mine else half - 1
-
     def z_stage(k, c):
         for way in (0, 1):
-            limit = z_limit(way, c)
+            limit = half - 1
 
             @pl.when((k >= 1) & (k <= limit))
             def _():
@@ -191,9 +198,14 @@
     offset = lax.broadcasted_iota(jnp.int32, (8, LANES), 0)
     column = offset + x
     column = jnp.where(column >= X, column - X, column)
-    expert_of = jnp.where(offset < X, z * X + column, -2).astype(jnp.float32)
+
+    def experts_at(dz):
+        return jnp.where(offset < X, lax.rem(z + dz + Z, Z) * X + column, -2).astype(jnp.float32)
 
     def build(r):
+        build_for(r, experts_at(0), pick.at[r], spread.at[r])
+
+    def build_for(r, expert_of, pick_ref, spread_ref):
         table = tables[r].astype(jnp.float32)
         named = jnp.zeros((8, LANES), jnp.float32)
         weight = jnp.zeros((8, LANES), jnp.float32)
@@ -209,8 +221,8 @@
             block = jnp.where(code[d : d + 1, :] == slot, 1.0, 0.0)
             parts.append(block)
             weighted.append(block * weight[d : d + 1, :])
-        pick[r] = jnp.concatenate(parts, axis=0).astype(jnp.bfloat16)
-        spread[r] = jnp.concatenate(weighted, axis=0).T.astype(jnp.bfloat16)
+        pick_ref[...] = jnp.concatenate(parts, axis=0).astype(jnp.bfloat16)
+        spread_ref[...] = jnp.concatenate(weighted, axis=0).T.astype(jnp.bfloat16)
 
     t_stage(jnp.int32(0))
     build(0)
@@ -247,9 +259,9 @@
                 ).astype(jnp.bfloat16)
         s_copy.start()
 
-    def x_copy(r, d):
+    def x_copy(r, d, c):
         rows = pl.ds(d * R, R)
-        return send(staged.at[r, :, rows, :], rows_in.at[r, tp, :, rows, :], x_send.at[r], x_recv.at[r], at_x(d))
+        return send(staged.at[r, c, rows, :], rows_in.at[r, tp, c, rows, :], x_send.at[r], x_recv.at[r], at_x(d))
 
     def c_copy(r):
         return send(rows_in.at[r, tp], rows_in.at[r, tp], c_send.at[r], c_recv.at[r], partner)
@@ -257,19 +269,56 @@
     def p_copy(r):
         return send(partial.at[r, other], partner_part.at[r], p_send.at[r], p_recv.at[r], partner)
 
-    def b_copy(r, d):
+    def b_copy(r, d, c):
         rows = pl.ds(d * R, R)
-        return send(total.at[r, :, rows, :], back.at[r, :, rows, :], b_send.at[r], b_recv.at[r], at_x(-d))
-
-    def select(r):
-        for c in range(nc):
-            chosen = jnp.dot(
-                pick[r, :, pl.ds(0, S)], gathered[r, c], preferred_element_type=jnp.float32
-            ).astype(jnp.bfloat16)
-            rows_in[r, tp, c, pl.ds(0, R), :] = chosen[:R]
-            staged[r, c] = chosen
+        return send(total.at[r, c, rows, :], back.at[r, c, rows, :], b_send.at[r], b_recv.at[r, c], at_x(-d))
+
+    def select(r, c):
+        chosen = jnp.dot(
+            pick[r, :, pl.ds(0, S)], gathered[r, c], preferred_element_type=jnp.float32
+        ).astype(jnp.bfloat16)
+        rows_in[r, tp, c, pl.ds(0, R), :] = chosen[:R]
+        staged[r, c] = chosen
         for d in range(1, X):
-            x_copy(r, d).start()
+            x_copy(r, d, c).start()
+
+    def far_row(way):
+        return half - 1 if way == 0 else Z - half + 1
+
+    def far_chunks(way):
+        return pl.ds(way * hc, hc)
+
+    def f_copy(way, d, c):
+        rows = pl.ds(d * R, R)
+        return send(
+            far_staged.at[way, c, rows, :],
+            rows_in.at[half, tp, way * hc + c, rows, :],
+            f_send.at[way],
+            x_recv.at[half],
+            at_far(1 - 2 * way, d),
+        )
+
+    def g_copy(way, d, c):
+        rows = pl.ds(d * R, R)
+        return send(
+            total.at[half, way * hc + c, rows, :],
+            far_back.at[way, c, rows, :],
+            g_send.at[way],
+            f_recv.at[way, c],
+            at_far(2 * way - 1, -d),
+        )
+
+    def select_far(c):
+        way = c // hc
+        far_staged[way, c - way * hc] = jnp.dot(
+            far_pick[way, :, pl.ds(0, S)], gathered[far_row(way), c], preferred_element_type=jnp.float32
+        ).astype(jnp.bfloat16)
+        for d in range(X):
+            f_copy(way, d, c - way * hc).start()
+
+    def hand_far():
+        send(rows_in.at[half, tp], rows_in.at[half, tp], f_send.at[0], x_recv.at[half], partner).wait_recv()
+        c_copy(half).start()
 
     rest = pl.ds(R, (X - 1) * R)
 
@@ -277,36 +326,44 @@
         send(staged.at[r, :, rest, :], rows_in.at[r, tp, :, rest, :], x_send.at[r], x_recv.at[r], at_x(1)).wait_recv()
         c_copy(r).start()
 
-    def expert(r):
-        send(rows_in.at[r, other], rows_in.at[r, other], c_send.at[r], c_recv.at[r], partner).wait_recv()
-        acc = jnp.zeros((X * R, 2 * F), jnp.float32)
+    def expert(rs):
+        M = X * R
+        for r in rs:
+            send(rows_in.at[r, other], rows_in.at[r, other], c_send.at[r], c_recv.at[r], partner).wait_recv()
+        acc = jnp.zeros((len(rs) * M, 2 * F), jnp.float32)
         for h in range(2):
             for c in range(nc):
-                acc = acc + jnp.dot(
-                    rows_in[r, h, c], w_in[pl.ds(h * H + c * W, W), :], preferred_element_type=jnp.float32
-                )
+                rows = jnp.concatenate([rows_in[r, h, c] for r in rs], axis=0)
+                acc = acc + jnp.dot(rows, w_in[pl.ds(h * H + c * W, W), :], preferred_element_type=jnp.float32)
         hidden = (jax.nn.silu(acc[:, :F]) * acc[:, F:]).astype(jnp.bfloat16)
         for h in range(2):
             for c in range(nc):
-                partial[r, h, c] = jnp.dot(
+                piece = jnp.dot(
                     hidden, w_out[:, pl.ds(h * H + c * W, W)], preferred_element_type=jnp.float32
                 ).astype(jnp.bfloat16)
-        p_copy(r).start()
+                for n, r in enumerate(rs):
+                    partial[r, h, c] = piece[n * M : (n + 1) * M]
+        for r in rs:
+            p_copy(r).start()
 
     def join(r):
         p_copy(r).wait_recv()
         for c in range(nc):
-            y = (partial[r, tp, c].astype(jnp.float32) + partner_part[r, c].astype(jnp.float32)).astype(jnp.bfloat16)
-            back[r, c, pl.ds(0, R), :] = y[:R]
-            total[r, c] = y
+            join_chunk(r, c)
+
+    def join_chunk(r, c):
+        y = (partial[r, tp, c].astype(jnp.float32) + partner_part[r, c].astype(jnp.float32)).astype(jnp.bfloat16)
+        back[r, c, pl.ds(0, R), :] = y[:R]
+        total[r, c] = y
 
     def hand_back(r):
-        for d in range(1, X):
-            b_copy(r, d).start()
+        for c in range(nc):
+            for d in range(1, X):
+                b_copy(r, d, c).start()
 
     def of_pair(stage, k, way, least=0):
         if way == 0:
-            @pl.when((k >= least) & (k <= half))
+            @pl.when((k >= least) & (k < half))
             def _():
                 stage(k)
         else:
@@ -315,47 +372,75 @@
                 stage(Z - k)
 
     def step(i, carry):
-        @pl.when(i <= half)
+        @pl.when(i < half)
         def _():
             t_stage(i)
 
-        z_stage(i, 0)
         of_pair(build, i, 0, 1)
         of_pair(build, i, 1, 1)
-        of_pair(select, i - 1, 0)
-        of_pair(select, i - 1, 1)
-        z_stage(i, 1)
-
-        @pl.when(i == 1)
+
+        @pl.when(i == half - 1)
         def _():
-            shared_hidden()
-
-        @pl.when(i == 2)
+            for way in (0, 1):
+                build_for(far_row(way), experts_at(1 - 2 * way), far_pick.at[way], far_spread.at[way])
+
+        for c in range(nc):
+            z_stage(i, c)
+
+            @pl.when(i == half - 1)
+            def _():
+                select_far(c)
+
+            of_pair(functools.partial(select, c=c), i, 0, 1)
+            of_pair(functools.partial(select, c=c), i, 1, 1)
+            if c == 1:
+
+                @pl.when(i == 2)
+                def _():
+                    for copy in expert_copies():
+                        copy.wait()
+                    expert([0])
+
+                @pl.when(i > 2)
+                def _():
+                    expert([i - 2, Z - i + 2])
+
+            if c == 2:
+                of_pair(join, i - 3, 0)
+                of_pair(join, i - 3, 1)
+
+        @pl.when(i == half)
         def _():
-            shared_partial()
-
-        @pl.when(i == 3)
-        def _():
-            for copy in expert_copies():
-                copy.wait()
-
-        of_pair(hand_over, i - 2, 0)
-        of_pair(hand_over, i - 2, 1)
-        of_pair(expert, i - 3, 0)
-        z_stage(i, 2)
-        of_pair(expert, i - 3, 1)
-        of_pair(join, i - 4, 0)
-        z_stage(i, 3)
-        of_pair(join, i - 4, 1)
-
-        @pl.when(i - 4 >= half - 1)
-        def _():
-            of_pair(hand_back, i - 4, 0)
-            of_pair(hand_back, i - 4, 1)
-
+            hand_far()
+
+        of_pair(hand_over, i - 1, 0)
+        of_pair(hand_over, i - 1, 1)
         return carry
 
-    lax.fori_loop(1, half + 5, step, 0)
+    for c in range(nc):
+        select(0, c)
+    lax.fori_loop(1, half + 1, step, 0)
+
+    last = (half - 1, half + 1, half)
+    expert(last)
+    join(half - 2)
+    if half > 2:
+        join(half + 2)
+    for r in last:
+        p_copy(r).wait_recv()
+    for c in range(nc):
+        for r in last:
+            join_chunk(r, c)
+        for d in range(X):
+            g_copy(c // hc, d, c - c // hc * hc).start()
+        for d in range(1, X):
+            b_copy(half - 1, d, c).start()
+            b_copy(half + 1, d, c).start()
+    hand_back(half - 2)
+    if half > 2:
+        hand_back(half + 2)
+    shared_hidden()
+    shared_partial()
 
     def r_copy(way, k, c):
         if way == 0:
@@ -365,43 +450,51 @@
     def share_of(r, c):
         return jnp.dot(spread[r, pl.ds(0, S), :], back[r, c], preferred_element_type=jnp.float32)
 
-    def back_wait(r):
-        send(total.at[r, :, rest, :], back.at[r, :, rest, :], b_send.at[r], b_recv.at[r], at_x(1)).wait_recv()
+    def back_wait(r, c):
+        send(total.at[r, c, rest, :], back.at[r, c, rest, :], b_send.at[r], b_recv.at[r, c], at_x(1)).wait_recv()
 
     def go_back(i, carry):
-        k = half - i
+        k = half - 1 - i
         of_pair(hand_back, k - 2, 0)
         of_pair(hand_back, k - 2, 1)
-        back_wait(k)
-
-        @pl.when(k < half)
-        def _():
-            back_wait(Z - k)
-
         for c in range(nc):
+            back_wait(k, c)
+            back_wait(Z - k, c)
+
+            @pl.when(k == half - 1)
+            def _():
+                way, at = c // hc, c - c // hc * hc
+                send(
+                    far_staged.at[way, at], far_back.at[way, at], g_send.at[way], f_recv.at[way, at], partner
+                ).wait_recv()
+
             for way in (0, 1):
-                limit = z_limit(way, c)
                 r = k if way == 0 else Z - k
-
-                @pl.when(k <= limit)
+                mine = share_of(r, c)
+
+                @pl.when(k == half - 1)
                 def _():
-                    mine = share_of(r, c)
-
-                    @pl.when(k == limit)
-                    def _():
-                        sums_out[r, c] = mine.astype(jnp.bfloat16)
-
-                    @pl.when(k < limit)
-                    def _():
-                        r_copy(way, k + 1, c).wait_recv()
-                        sums_out[r, c] = (mine + sums_in[r, c].astype(jnp.float32)).astype(jnp.bfloat16)
-
-                    r_copy(way, k, c).start()
+                    first = mine
+                    if c // hc == way:
+                        first = mine + jnp.dot(
+                            far_spread[way, pl.ds(0, S), :],
+                            far_back[way, c - way * hc],
+                            preferred_element_type=jnp.float32,
+                        )
+                    sums_out[r, c] = first.astype(jnp.bfloat16)
+
+                @pl.when(k < half - 1)
+                def _():
+                    r_copy(way, k + 1, c).wait_recv()
+                    sums_out[r, c] = (mine + sums_in[r, c].astype(jnp.float32)).astype(jnp.bfloat16)
+
+                r_copy(way, k, c).start()
         return carry
 
-    lax.fori_loop(0, half, go_back, 0)
-
-    back_wait(0)
+    lax.fori_loop(0, half - 1, go_back, 0)
+
+    for c in range(nc):
+        back_wait(0, c)
     s_copy.wait_recv()
     for c in range(nc):
         mine = share_of(0, c) + middle[:, own(c)].astype(jnp.float32)
@@ -417,30 +510,28 @@
 
     def drain(k, carry):
         for way in (0, 1):
-            @pl.when(k + 1 <= half - way)
-            def _():
-                t_copy(way, k).wait_send()
-
-        for c in range(nc):
-            for way in (0, 1):
-                limit = z_limit(way, c)
-
-                @pl.when(k + 1 <= limit)
-                def _():
-                    z_copy(way, k, c).wait_send()
-                    r_copy(way, k + 1, c).wait_send()
+            t_copy(way, k).wait_send()
+            for c in range(nc):
+                z_copy(way, k, c).wait_send()
+                r_copy(way, k + 1, c).wait_send()
         return carry
 
-    lax.fori_loop(0, half, drain, 0)
+    lax.fori_loop(0, half - 1, drain, 0)
 
     def drain_rows(r, carry):
-        send(staged.at[r, :, rest, :], rows_in.at[r, tp, :, rest, :], x_send.at[r], x_recv.at[r], at_x(1)).wait_send()
+        @pl.when(r != half)
+        def _():
+            send(staged.at[r, :, rest, :], rows_in.at[r, tp, :, rest, :], x_send.at[r], x_recv.at[r], at_x(1)).wait_send()
+            send(total.at[r, :, rest, :], back.at[r, :, rest, :], b_send.at[r], b_recv.at[r, 0], at_x(1)).wait_send()
+
         c_copy(r).wait_send()
         p_copy(r).wait_send()
-        send(total.at[r, :, rest, :], back.at[r, :, rest, :], b_send.at[r], b_recv.at[r], at_x(1)).wait_send()
         return carry
 
     lax.fori_loop(0, Z, drain_rows, 0)
+    for way in (0, 1):
+        send(far_staged.at[way], far_back.at[way], f_send.at[way], f_recv.at[way, 0], partner).wait_send()
+        send(total.at[half, far_chunks(way)], far_back.at[way], g_send.at[way], f_recv.at[way, 0], partner).wait_send()
 
 
 def layer(mixed, tokens, gain, routes, shares, sgate, sup, sdown, gate, up, down):
@@ -492,6 +583,10 @@
             pltpu.VMEM((Z, nc, X * R, W), bf),
             pltpu.VMEM((Z + 1, nc, S, W), bf),
             pltpu.VMEM((Z, nc, S, W), bf),
+            pltpu.VMEM((2, X * R, LANES), bf),
+            pltpu.VMEM((2, LANES, X * R), bf),
+            pltpu.VMEM((2, nc // 2, X * R, W), bf),
+            pltpu.VMEM((2, nc // 2, X * R, W), bf),
             dma((12,)),
             dma((2,)),
             dma((2,)),
@@ -506,9 +601,12 @@
             dma((Z,)),
             dma((Z,)),
             dma((Z,)),
-            dma((Z,)),
+            dma((Z, nc)),
             dma((Z, nc)),
             dma((Z + 1, nc)),
+            dma((2,)),
+            dma((2, nc // 2)),
+            dma((2,)),
         ],
         compiler_params=pltpu.CompilerParams(
             collective_id=0, has_side_effects=True, vmem_limit_bytes=VMEM_ALL

time: 126 us -> 118 us (0.937)
  Pallas kernels: 124 us -> 115 us
    pallas_call x1, Pallas kernels: 119 us -> 110 us  [layer(): pl.pallas_call(functools.partial(layer_kernel, (Z, X, S, H, R, nc, top)),...]
where the time goes in v4:
time: 118 us
  Pallas kernels  115 us (97%)
  local copies, waits for them, and re-layouts  1.62 us (1%)
    pallas_call x1, Pallas kernels, layer(): pl.pallas_call(functools.partial(layer_kernel, (Z, X, S, H, R, nc, top)),...  110 us
    pallas_call x1, Pallas kernels, mixer(): pl.pallas_call(mixer_kernel, out_shape=(jax.ShapeDtypeStruct((S, D), jnp....  4.92 us

profile of v4, /device:TPU:40, one launch (start us, length us, event | category | flops | bytes accessed | tf_op | source)
XLA Modules:
  0.0 117.5 jit_solution(10169787751816112634)
XLA Ops:
  0.6 4.9 %mixer.1 = (bf16[96,2048]{1,0:T(8,128)(2,1)}, f32[2,96,2048]{2,1,0:T(8,128)}) custom-call(bf16[96,2048]{1,0:T(8,128)(2,1)} %tokens_hbm.3, f32[2,96,2048]{2,1,0:T(8,128)} %prior_hbm.1, f32[1,2048]{1,0:T(1,128)} %bitcast.12, bf16[2048,512]{1,0:T(8,128)(2,1)} %weight_hbm.1, f32[32,64]{1,0:T(8,128)} %decay_hbm.1, f32[32,64]{1,0:T(8,128)} %freq_hbm.1, ...), custom_call_target="tpu_custom_call" | custom-call | tf_op jit(solution)/shard_map/mixer/pallas_call | solution.py:767
  5.6 110.4 %layer.1 = bf16[96,1024]{1,0:T(8,128)(2,1)} custom-call(bf16[96,2048]{1,0:T(8,128)(2,1)} %get-tuple-element.4.mixed_hbm, bf16[96,2048]{1,0:T(8,128)(2,1)} %tokens_hbm.3, f32[1,2048]{1,0:T(1,128)} %bitcast.13, s32[6,96]{1,0:T(8,128)} %bitcast.14, f32[6,96]{1,0:T(8,128)} %bitcast.15, bf16[2048,256]{1,0:T(8,128)(2,1)} %sgate_hbm.1, bf16[2048,256]{1,0:T(8,128)(2,1)} %sup_hbm.1, ...), custom_call_target="tpu_custom_call" | custom-call | tf_op jit(solution)/shard_map/layer/pallas_call | solution.py:552
  115.9 1.6 %copy.23 = bf16[96,1024]{1,0:T(8,128)(2,1)} copy(bf16[96,1024]{1,0:T(8,128)(2,1)} %layer.1) | data formatting | bytes 393216

commit v5 on v4

--- a/solution.py
+++ b/solution.py
@@ -81,6 +81,8 @@
     f_send,
     f_recv,
     g_send,
+    near_sem,
+    far_sem,
 ):
     Z, X, S, H, R, nc, top = cfg
     W = H // nc
@@ -140,7 +142,8 @@
         copy.start()
 
     barrier = pltpu.get_barrier_semaphore()
-    for device in (*[at_far(s, d) for s in (1, -1) for d in range(X)], *[at_x(d) for d in range(1, X)], partner):
+    beside = (at_z(1), at_z(-1), at_x(1), at_x(-1))
+    for device in (*beside, partner):
         pl.semaphore_signal(barrier, inc=1, device_id=device, device_id_type=MESH)
 
     table[...] = jnp.where(lax.broadcasted_iota(jnp.int32, (16, LANES), 0) < 8, -1.0, 0.0)
@@ -151,7 +154,10 @@
     tables[0] = table[...].astype(jnp.bfloat16)
     for copy in (*shared_copies(), *expert_copies()):
         copy.start()
-    pl.semaphore_wait(barrier, 3 * X)
+    pl.semaphore_wait(barrier, 5)
+
+    for device in beside:
+        pl.semaphore_signal(near_sem, inc=1, device_id=device, device_id_type=MESH)
 
     mixed_copy = send(mixed, mixed_in, m_sem.at[0], m_sem.at[1], partner)
     mixed_copy.start()
@@ -234,14 +240,15 @@
     middle[...] = (tokens_ref[...].astype(jnp.float32) + both).astype(jnp.bfloat16)
     values = middle[...].astype(jnp.float32)
     factor = lax.rsqrt(jnp.mean(values * values, axis=-1, keepdims=True) + norm_eps)
-    normed[...] = (values * factor * gain_ref[...]).astype(jnp.bfloat16)
 
     def own(c):
         return pl.ds(pl.multiple_of(tp * H + c * W, W), W)
 
     for c in range(nc):
-        gathered[0, c] = normed[:, own(c)]
+        mine = middle[:, own(c)].astype(jnp.float32) * factor * gain_ref[:, own(c)]
+        gathered[0, c] = mine.astype(jnp.bfloat16)
         z_stage(jnp.int32(0), c)
+    normed[...] = (values * factor * gain_ref[...]).astype(jnp.bfloat16)
 
     def shared_hidden():
         for copy in shared_copies():
@@ -336,15 +343,15 @@
                 rows = jnp.concatenate([rows_in[r, h, c] for r in rs], axis=0)
                 acc = acc + jnp.dot(rows, w_in[pl.ds(h * H + c * W, W), :], preferred_element_type=jnp.float32)
         hidden = (jax.nn.silu(acc[:, :F]) * acc[:, F:]).astype(jnp.bfloat16)
-        for h in range(2):
+        for h in (other, tp):
             for c in range(nc):
-                piece = jnp.dot(
-                    hidden, w_out[:, pl.ds(h * H + c * W, W)], preferred_element_type=jnp.float32
-                ).astype(jnp.bfloat16)
+                cols = pl.ds(pl.multiple_of(h * H + c * W, W), W)
+                piece = jnp.dot(hidden, w_out[:, cols], preferred_element_type=jnp.float32).astype(jnp.bfloat16)
                 for n, r in enumerate(rs):
                     partial[r, h, c] = piece[n * M : (n + 1) * M]
-        for r in rs:
-            p_copy(r).start()
+            if h is other:
+                for r in rs:
+                    p_copy(r).start()
 
     def join(r):
         p_copy(r).wait_recv()
@@ -381,6 +388,7 @@
 
         @pl.when(i == half - 1)
         def _():
+            pl.semaphore_wait(far_sem, 2)
             for way in (0, 1):
                 build_for(far_row(way), experts_at(1 - 2 * way), far_pick.at[way], far_spread.at[way])
 
@@ -417,6 +425,9 @@
         of_pair(hand_over, i - 1, 1)
         return carry
 
+    pl.semaphore_wait(near_sem, 4)
+    for device in beside[:2]:
+        pl.semaphore_signal(far_sem, inc=1, device_id=device, device_id_type=MESH)
     for c in range(nc):
         select(0, c)
     lax.fori_loop(1, half + 1, step, 0)
@@ -607,9 +618,11 @@
             dma((2,)),
             dma((2, nc // 2)),
             dma((2,)),
+            pltpu.SemaphoreType.REGULAR,
+            pltpu.SemaphoreType.REGULAR,
         ],
         compiler_params=pltpu.CompilerParams(
-            collective_id=0, has_side_effects=True, vmem_limit_bytes=VMEM_ALL
+            collective_id=0, has_side_effects=True, vmem_limit_bytes=56300000
         ),
         name="layer",
     )(mixed, tokens, gain[None, :], routes.T, shares.T, sgate, sup, sdown, gate, up, down)

time: 118 us -> 115 us (0.975)
  Pallas kernels: 115 us -> 113 us
    pallas_call x1, Pallas kernels: 110 us -> 108 us  [layer(): pl.pallas_call(functools.partial(layer_kernel, (Z, X, S, H, R, nc, top)),...]
where the time goes in v5:
time: 115 us
  Pallas kernels  113 us (98%)
    pallas_call x1, Pallas kernels, layer(): pl.pallas_call(functools.partial(layer_kernel, (Z, X, S, H, R, nc, top)),...  108 us
    pallas_call x1, Pallas kernels, mixer(): pl.pallas_call(mixer_kernel, out_shape=(jax.ShapeDtypeStruct((S, D), jnp....  4.93 us

profile of v5, /device:TPU:40, one launch (start us, length us, event | category | flops | bytes accessed | tf_op | source)
XLA Modules:
  0.0 114.8 jit_solution(17458328533290830988)
XLA Ops:
  0.6 0.0 copy-start
  0.6 0.0 copy-start.1
  0.7 0.0 copy-start.2
  0.7 4.9 %mixer.1 = (bf16[96,2048]{1,0:T(8,128)(2,1)}, f32[2,96,2048]{2,1,0:T(8,128)}) custom-call(bf16[96,2048]{1,0:T(8,128)(2,1)} %tokens_hbm.3, f32[2,96,2048]{2,1,0:T(8,128)} %prior_hbm.1, f32[1,2048]{1,0:T(1,128)} %bitcast.15, bf16[2048,512]{1,0:T(8,128)(2,1)} %weight_hbm.1, f32[32,64]{1,0:T(8,128)} %decay_hbm.1, f32[32,64]{1,0:T(8,128)} %freq_hbm.1, ...), custom_call_target="tpu_custom_call" | custom-call | tf_op jit(solution)/shard_map/mixer/pallas_call | solution.py:780
  5.6 0.0 copy-done
  5.6 0.0 copy-done.1
  5.6 0.0 copy-done.2
  5.6 108.4 %layer.1 = bf16[96,1024]{1,0:T(8,128)(2,1)S(1)} custom-call(bf16[96,2048]{1,0:T(8,128)(2,1)} %get-tuple-element.4.mixed_hbm, bf16[96,2048]{1,0:T(8,128)(2,1)} %tokens_hbm.3, f32[1,2048]{1,0:T(1,128)S(1)} %bitcast.10, s32[6,96]{1,0:T(8,128)S(1)} %bitcast.11, f32[6,96]{1,0:T(8,128)S(1)} %bitcast.12, bf16[2048,256]{1,0:T(8,128)(2,1)} %sgate_hbm.1, ...), custom_call_target="tpu_custom_call" | custom-call | tf_op jit(solution)/shard_map/layer/pallas_call | solution.py:563
  114.1 0.7 copy.23
Async XLA Ops:
  0.6 5.0 %copy-start = (f32[2048]{0:T(1024)S(1)}, f32[2048]{0:T(1024)}, u32[]{:S(2)}) copy-start(f32[2048]{0:T(1024)} %param.31) | copy-start | bytes 24580
  0.6 5.0 %copy-start.1 = (s32[96,6]{0,1:T(8,128)S(1)}, s32[96,6]{0,1:T(8,128)}, u32[]{:S(2)}) copy-start(s32[96,6]{0,1:T(8,128)} %param.38) | copy-start | bytes 6916
  0.7 5.0 %copy-start.2 = (f32[96,6]{0,1:T(8,128)S(1)}, f32[96,6]{0,1:T(8,128)}, u32[]{:S(2)}) copy-start(f32[96,6]{0,1:T(8,128)} %param.39) | copy-start | bytes 6916

commit v6 on v5

--- a/solution.py
+++ b/solution.py
@@ -335,13 +335,15 @@
 
     def expert(rs):
         M = X * R
-        for r in rs:
-            send(rows_in.at[r, other], rows_in.at[r, other], c_send.at[r], c_recv.at[r], partner).wait_recv()
         acc = jnp.zeros((len(rs) * M, 2 * F), jnp.float32)
-        for h in range(2):
+        for h in (tp, other):
+            if h is other:
+                for r in rs:
+                    send(rows_in.at[r, other], rows_in.at[r, other], c_send.at[r], c_recv.at[r], partner).wait_recv()
             for c in range(nc):
                 rows = jnp.concatenate([rows_in[r, h, c] for r in rs], axis=0)
-                acc = acc + jnp.dot(rows, w_in[pl.ds(h * H + c * W, W), :], preferred_element_type=jnp.float32)
+                depth = pl.ds(pl.multiple_of(h * H + c * W, W), W)
+                acc = acc + jnp.dot(rows, w_in[depth, :], preferred_element_type=jnp.float32)
         hidden = (jax.nn.silu(acc[:, :F]) * acc[:, F:]).astype(jnp.bfloat16)
         for h in (other, tp):
             for c in range(nc):

time: 115 us -> 115 us (level)
  no operation moved by 1% of the time
where the time goes in v6:
time: 115 us
  Pallas kernels  113 us (98%)
    pallas_call x1, Pallas kernels, layer(): pl.pallas_call(functools.partial(layer_kernel, (Z, X, S, H, R, nc, top)),...  108 us
    pallas_call x1, Pallas kernels, mixer(): pl.pallas_call(mixer_kernel, out_shape=(jax.ShapeDtypeStruct((S, D), jnp....  4.93 us

profile of v6, /device:TPU:40, one launch (start us, length us, event | category | flops | bytes accessed | tf_op | source)
XLA Modules:
  0.0 114.6 jit_solution(4145248777055224673)
XLA Ops:
  0.6 0.0 copy-start
  0.6 0.0 copy-start.1
  0.7 0.0 copy-start.2
  0.7 4.9 %mixer.1 = (bf16[96,2048]{1,0:T(8,128)(2,1)}, f32[2,96,2048]{2,1,0:T(8,128)}) custom-call(bf16[96,2048]{1,0:T(8,128)(2,1)} %tokens_hbm.3, f32[2,96,2048]{2,1,0:T(8,128)} %prior_hbm.1, f32[1,2048]{1,0:T(1,128)} %bitcast.15, bf16[2048,512]{1,0:T(8,128)(2,1)} %weight_hbm.1, f32[32,64]{1,0:T(8,128)} %decay_hbm.1, f32[32,64]{1,0:T(8,128)} %freq_hbm.1, ...), custom_call_target="tpu_custom_call" | custom-call | tf_op jit(solution)/shard_map/mixer/pallas_call | solution.py:782
  5.6 0.0 copy-done
  5.6 0.0 copy-done.1
  5.6 0.0 copy-done.2
  5.6 108.3 %layer.1 = bf16[96,1024]{1,0:T(8,128)(2,1)S(1)} custom-call(bf16[96,2048]{1,0:T(8,128)(2,1)} %get-tuple-element.4.mixed_hbm, bf16[96,2048]{1,0:T(8,128)(2,1)} %tokens_hbm.3, f32[1,2048]{1,0:T(1,128)S(1)} %bitcast.10, s32[6,96]{1,0:T(8,128)S(1)} %bitcast.11, f32[6,96]{1,0:T(8,128)S(1)} %bitcast.12, bf16[2048,256]{1,0:T(8,128)(2,1)} %sgate_hbm.1, ...), custom_call_target="tpu_custom_call" | custom-call | tf_op jit(solution)/shard_map/layer/pallas_call | solution.py:565
  114.0 0.7 copy.23
Async XLA Ops:
  0.6 5.0 %copy-start = (f32[2048]{0:T(1024)S(1)}, f32[2048]{0:T(1024)}, u32[]{:S(2)}) copy-start(f32[2048]{0:T(1024)} %param.31) | copy-start | bytes 24580
  0.6 5.0 %copy-start.1 = (s32[96,6]{0,1:T(8,128)S(1)}, s32[96,6]{0,1:T(8,128)}, u32[]{:S(2)}) copy-start(s32[96,6]{0,1:T(8,128)} %param.38) | copy-start | bytes 6916
  0.7 5.0 %copy-start.2 = (f32[96,6]{0,1:T(8,128)S(1)}, f32[96,6]{0,1:T(8,128)}, u32[]{:S(2)}) copy-start(f32[96,6]{0,1:T(8,128)} %param.39) | copy-start | bytes 6916
